TPU v7x, 512 devices: a whole 4x4x16 slice. The times are simulated.
512 devices in a mesh: sp: 64 (over z, y), tp: 8 (over x, core).
Axes of the slice: x: 4, y: 4, z: 16, core: 2. Of those that a mesh axis runs over, the one named last changes fastest.
Arguments:
- tokens: bfloat16 [24576, 4096], P(('sp', 'tp')), may hold values from -6 to 6
- norm_gain: float32 [4096], replicated, may hold values from 0.1 to 1.9
- conv_val_w: bfloat16 [4096, 1024], P('sp', 'tp'), may hold values from -0.09375 to 0.09375
- conv_gate_w: bfloat16 [4096, 1024], P('sp', 'tp'), may hold values from -0.09375 to 0.09375
- rec_gate_w: bfloat16 [4096, 1536], P('sp', 'tp'), may hold values from -0.09375 to 0.09375
- rec_in_w: bfloat16 [4096, 1536], P('sp', 'tp'), may hold values from -0.09375 to 0.09375
- conv_taps: bfloat16 [31, 1024], P(None, 'tp'), may hold values from -3 to 3
- conv_bias: float32 [1024], P('tp'), may hold values from 1 to 15
- conv_gain: float32 [1024], P('tp'), may hold values from 0.1 to 1.9
- short_taps: bfloat16 [4, 1536], P(None, 'tp'), may hold values from -3 to 3
- decay_map: bfloat16 [24, 64, 64], P('tp'), may hold values from -0.75 to 0.75
- input_map: bfloat16 [24, 64, 64], P('tp'), may hold values from -0.75 to 0.75
- decay_base: float32 [1536], P('tp'), may hold values from 3.5 to 17
- decay_jump: float32 [24576, 1536], P('sp', 'tp'), may hold values from -1.5 to 0
- out_conv_w: bfloat16 [1024, 4096], P('tp', 'sp'), may hold values from -0.125 to 0.125
- out_rec_w: bfloat16 [1536, 4096], P('tp', 'sp'), may hold values from -0.125 to 0.125
Outputs:
- mixed: bfloat16 [24576, 4096], P(('sp', 'tp'))
All inputs are finite; a program needn't handle non-finite values.
Results may differ from a plain program's by a relative error of at most 0.015.
Values may be sent and summed in bfloat16 or wider, within the bound.
A program may use at most 64 MiB of HBM per device.

v0:
```python
import jax
import jax.numpy as jnp
from jax import lax
from jax.sharding import PartitionSpec as P

CONV_WIDTH = 1024


RATE_SCALE = 8.0


def sent_together(arrays, axis, dim, along):
    widths = [a.shape[along] for a in arrays]
    both = jnp.concatenate(arrays, axis=along)
    out = lax.all_gather(both, axis, axis=dim, tiled=True)
    return tuple(jnp.split(out, [sum(widths[:k]) for k in range(1, len(widths))], axis=along))


def passed_along(value, axis, by):
    count = lax.axis_size(axis)
    pairs = [(i, i + by) for i in range(count) if 0 <= i + by < count]
    return lax.ppermute(value, axis, pairs)


def sent_to_all(value, axis):
    count = lax.axis_size(axis)
    return lax.all_to_all(
        jnp.broadcast_to(value[None], (count, *value.shape)), axis, 0, 0, tiled=True
    )


def of_everyone(value, axis):
    return sent_to_all(value, axis).sum(axis=0)


def together(arrays, axis):
    ends = [0]
    for a in arrays:
        ends.append(ends[-1] + a.size)
    so_far = of_everyone(jnp.concatenate([a.ravel() for a in arrays]), axis)
    return tuple((so_far[b:e].reshape(a.shape) for a, b, e in zip(arrays, ends, ends[1:])))


def gathered_once(value, axis):
    leaves = jax.tree.leaves(value)
    sequence = sorted(range(len(leaves)), key=lambda k: -leaves[k].size)
    width = (1, *leaves[sequence[0]].shape)[-1]
    lines = [
        jnp.pad(leaves[k].reshape(-1), (0, -leaves[k].size % width)).reshape(-1, width)
        for k in sequence
    ]
    both, at, found = (sent_to_all(jnp.concatenate(lines), axis), 0, {})
    for k, line in zip(sequence, lines):
        piece = both[:, at : at + len(line)].reshape(len(both), -1)
        found[k] = piece[:, : leaves[k].size].reshape(-1, *leaves[k].shape)
        at += len(line)
    numbers = iter(range(len(leaves)))
    return jax.tree.map(lambda _: found[next(numbers)], value)


def folded_in_pairs(pieces, combine):
    while len(jax.tree.leaves(pieces)[0]) > 1:
        pieces = jax.vmap(combine)(
            *(jax.tree.map(lambda part: part[side::2], pieces) for side in (0, 1))
        )
    return jax.tree.map(lambda part: part[0], pieces)


def carried_in(value, axis, combine, identity):
    count, mine = (lax.axis_size(axis), lax.axis_index(axis))
    passed = jnp.arange(count) < mine

    def kept(part, zero, own):
        part = jnp.where(
            passed.reshape(-1, *(1 for _ in own.shape)), part, jnp.asarray(zero, own.dtype)
        )
        return part

    pieces = gathered_once(value, axis)
    return folded_in_pairs(jax.tree.map(kept, pieces, identity, value), combine)


def gather_turned(arrays, axis, dims):
    turned = [jnp.moveaxis(a, dim, 0) for a, dim in zip(arrays, dims)]
    widths = [t[0].size for t in turned]
    both = jnp.concatenate([t.reshape(-1, w) for t, w in zip(turned, widths)], axis=1)
    out = lax.all_gather(both, axis, axis=0, tiled=True)
    pieces = jnp.split(out, [sum(widths[:k]) for k in range(1, len(widths))], axis=1)
    return tuple(
        (
            jnp.moveaxis(b.reshape(-1, *t.shape[1:]), 0, dim)
            for b, t, dim in zip(pieces, turned, dims)
        )
    )


def norm_rows(values, gain):
    widened = values.astype(jnp.float32)
    inverse = lax.rsqrt(jnp.mean(widened * widened, axis=-1, keepdims=True) + 1e-06)
    return (widened * inverse * gain).astype(jnp.bfloat16)


def causal_window(edge, current, weights):
    extended = jnp.concatenate([edge, current], axis=0).astype(jnp.float32)
    taps_wide = weights.astype(jnp.float32)
    length = current.shape[0]
    result = jnp.zeros((length, current.shape[1]), jnp.float32)
    for lag_index in range(weights.shape[0]):
        result = result + taps_wide[lag_index][None, :] * extended[lag_index : lag_index + length]
    return result


def chain_step(earlier, latter):
    return (earlier[0] * latter[0], latter[0] * earlier[1] + latter[1])


def glu_of(conv_val, conv_gate):
    return (conv_val.astype(jnp.float32) * jax.nn.sigmoid(conv_gate.astype(jnp.float32))).astype(
        jnp.bfloat16
    )


def shards(
    tokens,
    norm_gain,
    conv_val_w,
    conv_gate_w,
    rec_gate_w,
    rec_in_w,
    conv_taps,
    conv_bias,
    conv_gain,
    short_taps,
    decay_map,
    input_map,
    decay_base,
    decay_jump,
    out_conv_w,
    out_rec_w,
):
    conv_cols = conv_val_w.shape[1]
    rec_cols = rec_in_w.shape[1]
    conv_lags = conv_taps.shape[0] - 1
    short_lags = short_taps.shape[0] - 1
    normed = norm_rows(tokens, norm_gain)
    val_full, gate_full, rgate_full, rin_full = sent_together(
        (conv_val_w, conv_gate_w, rec_gate_w, rec_in_w), "sp", 0, 1
    )
    joined = jnp.concatenate([val_full, gate_full, rgate_full, rin_full], axis=1)
    projected = jnp.dot(
        lax.all_gather(normed, "tp", axis=0, tiled=True), joined, preferred_element_type=jnp.float32
    ).astype(jnp.bfloat16)
    glu = glu_of(projected[:, :conv_cols], projected[:, conv_cols : 2 * conv_cols])
    rec_gate = projected[:, 2 * conv_cols : 2 * conv_cols + rec_cols]
    rec_in = projected[:, 2 * conv_cols + rec_cols :]
    conv_edge, rec_edge = passed_along((glu[-conv_lags:], rec_in[-short_lags:]), "sp", 1)
    filtered = causal_window(conv_edge, glu, conv_taps) + conv_bias[None, :]
    row_total, row_squares = together(
        (jnp.sum(filtered, axis=1), jnp.sum(filtered * filtered, axis=1)), "tp"
    )
    row_mean = row_total / CONV_WIDTH
    spread = row_squares / CONV_WIDTH - row_mean * row_mean
    centered = filtered - row_mean[:, None]
    conv_out = jax.nn.silu(centered * lax.rsqrt(spread + 1e-05)[:, None] * conv_gain).astype(
        jnp.bfloat16
    )
    smoothed = causal_window(rec_edge, rec_in, short_taps).astype(jnp.bfloat16)
    length = smoothed.shape[0]
    grouped = smoothed.reshape(length, decay_map.shape[0], decay_map.shape[1])
    retain = jax.nn.sigmoid(
        jnp.einsum("thi,hio->tho", grouped, decay_map, preferred_element_type=jnp.float32).reshape(
            length, rec_cols
        )
    )
    admit = jax.nn.sigmoid(
        jnp.einsum("thi,hio->tho", grouped, input_map, preferred_element_type=jnp.float32).reshape(
            length, rec_cols
        )
    )
    log_decay = -RATE_SCALE * retain * jax.nn.softplus(-decay_base)[None, :] + decay_jump
    decay = jnp.exp(log_decay)
    inflow = jnp.sqrt(-jnp.expm1(2.0 * log_decay)) * admit * smoothed.astype(jnp.float32)
    products, local_state = lax.associative_scan(chain_step, (decay, inflow), axis=0)
    entering = carried_in(
        (products[-1], local_state[-1]),
        "sp",
        chain_step,
        (jnp.ones((rec_cols,), jnp.float32), jnp.zeros((rec_cols,), jnp.float32)),
    )
    state = local_state + products * entering[1][None, :]
    rec_out = (jax.nn.gelu(rec_gate.astype(jnp.float32)) * state).astype(jnp.bfloat16)
    conv_full, rec_full = gather_turned((out_conv_w, out_rec_w), "sp", (1, 1))
    return lax.psum_scatter(
        (
            jnp.dot(conv_out, conv_full, preferred_element_type=jnp.float32)
            + jnp.dot(rec_out, rec_full, preferred_element_type=jnp.float32)
        ).astype(jnp.bfloat16),
        "tp",
        scatter_dimension=0,
        tiled=True,
    )


def solution(mesh):
    in_specs = (
        P(("sp", "tp"), None),
        P(),
        P("sp", "tp"),
        P("sp", "tp"),
        P("sp", "tp"),
        P("sp", "tp"),
        P(None, "tp"),
        P("tp"),
        P("tp"),
        P(None, "tp"),
        P("tp", None, None),
        P("tp", None, None),
        P("tp"),
        P("sp", "tp"),
        P("tp", "sp"),
        P("tp", "sp"),
    )
    out_specs = P(("sp", "tp"), None)
    return jax.shard_map(shards, mesh=mesh, in_specs=in_specs, out_specs=out_specs, check_vma=False)
```

profile of v0, /device:TPU:1, one launch (start us, length us, event | category | flops | bytes accessed | tf_op | source)
XLA Modules:
  0.0 399.2 jit_solution(15747724890955525391)
XLA Ops:
  6.5 1.2 fusion.9
  7.7 1.9 fusion.11
  9.7 1.5 pad_maximum_fusion.4
  11.3 1.4 pad_maximum_fusion.5
  12.7 0.7 convert_element_type.48
  13.5 0.7 fusion.78
  14.2 0.8 fusion.91
  15.0 1.1 copy.48
  16.1 34.7 %all-gather.4.cloned.1.call-done = bf16[384,4096]{1,0:T(8,128)(2,1)} async-done(((bf16[48,4096]{1,0:T(8,128)(2,1)}), bf16[384,4096]{1,0:T(8,128)(2,1)}) %all-gather.4.cloned.1.call-update) | async-done | bytes 3145744 | tf_op jit(solution)/shard_map/all_gather | solution.py:151
  50.9 142.2 %all-gather.6.cloned.1.call-done = bf16[4096,640]{1,0:T(8,128)(2,1)} async-done(((bf16[64,640]{1,0:T(8,128)(2,1)}), bf16[4096,640]{1,0:T(8,128)(2,1)}) %all-gather.6.cloned.1.call-update) | async-done | bytes 5242896 | tf_op jit(solution)/shard_map/all_gather | solution.py:15
  193.0 6.0 %convolution_convert_fusion = bf16[384,640]{1,0:T(8,128)(2,1)S(1)} fusion(bf16[384,4096]{1,0:T(8,128)(2,1)} %all-gather.4.cloned.1.call-done, bf16[4096,640]{1,0:T(8,128)(2,1)} %all-gather.6.cloned.1.call-done), kind=kOutput, calls=%fused_computation.2 | convolution fusion | flops 2013511680 | bytes 8880128 | tf_op jit(solution)/shard_map/dot_general | solution.py:150
  199.1 0.1 slice.804
  199.2 1.9 collective-permute-start.1
  201.1 0.1 multiply_convert_fusion.1
  201.1 0.1 slice.805
  201.3 2.8 collective-permute-start
  204.2 0.2 fusion.20
  204.4 0.1 copy.45
  204.5 0.3 fusion.3
  204.8 0.2 copy.50
  205.0 0.3 fusion.6
  205.3 0.2 copy.47
  205.4 0.5 convert_multiply_fusion.5
  205.9 0.3 slice.694
  206.3 0.2 slice.638
  206.4 0.2 slice.637
  206.6 0.2 slice.640
  206.8 0.2 slice.636
  206.9 0.3 slice.635
  207.3 0.1 multiply_add_fusion.1
  207.3 0.1 slice.692
  207.6 0.1 slice.641
  209.7 0.1 fusion.24
  209.8 0.1 pad.128
  210.2 0.1 copy-done.8
  210.3 0.8 fusion.84
  211.1 0.6 broadcast_in_dim.18
  211.7 14.7 %all-to-all-start = ((f32[8,1,768]{2,1,0:T(1,128)}), f32[8,1,768]{2,1,0:T(1,128)S(1)}, u32[]{:S(2)}, u32[]{:S(2)}) async-start(f32[8,1,768]{2,1,0:T(1,128)} %broadcast_in_dim.18), calls=%async_computation | async-start | bytes 49152 | tf_op jit(solution)/shard_map/all_to_all | solution.py:27
  226.4 4.7 %all-to-all-done = f32[8,1,768]{2,1,0:T(1,128)S(1)} async-done(((f32[8,1,768]{2,1,0:T(1,128)}), f32[8,1,768]{2,1,0:T(1,128)S(1)}, u32[]{:S(2)}, u32[]{:S(2)}) %all-to-all-start) | async-done | bytes 24608 | tf_op jit(solution)/shard_map/all_to_all | solution.py:27
  231.1 0.7 broadcast_in_dim.20
  231.8 11.0 %all-to-all-start.1 = ((f32[64,2,192]{2,1,0:T(2,128)}), f32[64,2,192]{2,1,0:T(2,128)S(1)}, u32[]{:S(2)}, u32[]{:S(2)}) async-start(f32[64,2,192]{2,1,0:T(2,128)} %broadcast_in_dim.20), calls=%async_computation.1 | async-start | bytes 262144 | tf_op jit(solution)/shard_map/all_to_all | solution.py:27
  242.8 0.2 reduce-scatter.2.cloned.1.call-start
  243.0 91.8 %all-gather.8.cloned.1.call-done = bf16[4096,320]{1,0:T(8,128)(2,1)} async-done(((bf16[64,320]{1,0:T(8,128)(2,1)}), bf16[4096,320]{1,0:T(8,128)(2,1)}) %all-gather.8.cloned.1.call-update) | async-done | bytes 2621456 | tf_op jit(solution)/shard_map/all_gather | solution.py:87
  334.9 5.1 %fusion.7 = f32[384,4096]{1,0:T(8,128)} fusion(bf16[4096,320]{1,0:T(8,128)(2,1)} %all-gather.8.cloned.1.call-done, f32[384,128]{1,0:T(8,128)S(1)} %get-tuple-element.11, f32[128]{0:T(128)S(1)} %copy-done.7, f32[384]{0:T(512)S(1)} %get-tuple-element.86, f32[384]{0:T(512)S(1)} %get-tuple-element.85), kind=kOutput, calls=%fused_computation.11 | convolution fusion | flops 403046400 | bytes 7540224 | tf_op jit(solution)/shard_map/dot_general | solution.py:195
  339.9 0.1 fusion.86
  340.0 0.1 fusion.68
  340.6 6.1 %add_convert_fusion = bf16[384,4096]{1,0:T(8,128)(2,1)} fusion(f32[384,4096]{1,0:T(8,128)} %fusion.7, bf16[4096,320]{1,0:T(8,128)(2,1)S(1)} %copy-done.1, f32[384,192]{1,0:T(8,128)} %copy-done.2, f32[384,192]{1,0:T(8,128)} %copy-done.5, f32[384,192]{1,0:T(8,128)} %copy-done.3, f32[384,192]{1,0:T(8,128)} %copy-done.4, bf16[384,640]{1,0:T(8,128)(2,1)} %copy-done.6, ...), kind=kOutput, calls=%fused_computation | convolution fusion | flops 608231424 | bytes 13304832 | tf_op jit(solution)/shard_map/dot_general | solution.py:196
  346.8 45.8 %reduce-scatter.2.cloned.1.call-done = bf16[48,4096]{1,0:T(8,128)(2,1)} async-done(((bf16[384,4096]{1,0:T(8,128)(2,1)}), bf16[48,4096]{1,0:T(8,128)(2,1)}) %reduce-scatter.2.cloned.1.call-update) | async-done | bytes 393232 | tf_op jit(solution)/shard_map/reduce_scatter | solution.py:193
  (186 shorter events, 2.7 us)
Async XLA Ops:
  6.5 198.0 %copy-start = (bf16[3,64,64]{2,1,0:T(8,128)(2,1)S(1)}, bf16[3,64,64]{2,1,0:T(8,128)(2,1)}, u32[]{:S(2)}) copy-start(bf16[3,64,64]{2,1,0:T(8,128)(2,1)} %param.27) | copy-start | bytes 73732
  6.5 44.3 %all-gather.4.cloned.1.call-start = ((), (), s32[]{:S(2)}) async-start(), calls=%async_computation.3 | async-start | bytes 3538944 | tf_op jit(solution)/shard_map/all_gather | solution.py:151
  9.7 183.4 %all-gather.6.cloned.1.call-start = ((), (), s32[]{:S(2)}) async-start(), calls=%async_computation.4 | async-start | bytes 5324800 | tf_op jit(solution)/shard_map/all_gather | solution.py:15
  11.2 323.6 %all-gather.8.cloned.1.call-start = ((), (), s32[]{:S(2)}) async-start(), calls=%async_computation.5 | async-start | bytes 3194880 | tf_op jit(solution)/shard_map/all_gather | solution.py:87
  199.1 6.2 %copy-start.6 = (bf16[384,640]{1,0:T(8,128)(2,1)}, bf16[384,640]{1,0:T(8,128)(2,1)S(1)}, u32[]{:S(2)}) copy-start(bf16[384,640]{1,0:T(8,128)(2,1)S(1)} %convolution_convert_fusion) | copy-start | bytes 1474564
  199.1 5.9 %copy-start.9 = (bf16[3,64,64]{2,1,0:T(8,128)(2,1)S(1)}, bf16[3,64,64]{2,1,0:T(8,128)(2,1)}, u32[]{:S(2)}) copy-start(bf16[3,64,64]{2,1,0:T(8,128)(2,1)} %param.26) | copy-start | bytes 73732
  199.2 4.9 %collective-permute-start.1 = (bf16[3,192]{1,0:T(4,128)(2,1)S(1)}, bf16[3,192]{1,0:T(4,128)(2,1)S(1)}, u32[]{:S(2)}, u32[]{:S(2)}) collective-permute-start(bf16[3,192]{1,0:T(4,128)(2,1)S(1)} %slice.804), channel_id=1, source_target_pairs={{0,8},{8,16},{16,24},{24,32},{32,40},{40,48},{48,56},{56,64},{64,7... | collective-permute-start | bytes 3464 | tf_op jit(solution)/shard_map/ppermute | solution.py:22
  201.3 8.9 %collective-permute-start = (bf16[30,128]{1,0:T(8,128)(2,1)S(1)}, bf16[30,128]{1,0:T(8,128)(2,1)S(1)}, u32[]{:S(2)}, u32[]{:S(2)}) collective-permute-start(bf16[30,128]{1,0:T(8,128)(2,1)S(1)} %slice.740), channel_id=1, source_target_pairs={{0,8},{8,16},{16,24},{24,32},{32,40},{40,48},{48,56},{56,64},{64,7... | collective-permute-start | bytes 23048 | tf_op jit(solution)/shard_map/ppermute | solution.py:22
  209.6 0.7 copy-start.8
  209.9 1.1 copy-start.2
  210.0 1.0 copy-start.3
  210.1 1.0 copy-start.4
  210.1 0.9 copy-start.5
  210.3 124.6 %copy-start.7 = (f32[128]{0:T(128)S(1)}, f32[128]{0:T(128)}, u32[]{:S(2)}) copy-start(f32[128]{0:T(128)} %param.24) | copy-start | bytes 1540
  211.7 19.4 %all-to-all-start = ((f32[8,1,768]{2,1,0:T(1,128)}), f32[8,1,768]{2,1,0:T(1,128)S(1)}, u32[]{:S(2)}, u32[]{:S(2)}) async-start(f32[8,1,768]{2,1,0:T(1,128)} %broadcast_in_dim.18), calls=%async_computation | async-start | bytes 49152 | tf_op jit(solution)/shard_map/all_to_all | solution.py:27
  231.8 108.2 %all-to-all-start.1 = ((f32[64,2,192]{2,1,0:T(2,128)}), f32[64,2,192]{2,1,0:T(2,128)S(1)}, u32[]{:S(2)}, u32[]{:S(2)}) async-start(f32[64,2,192]{2,1,0:T(2,128)} %broadcast_in_dim.20), calls=%async_computation.1 | async-start | bytes 262144 | tf_op jit(solution)/shard_map/all_to_all | solution.py:27
  242.8 149.9 %reduce-scatter.2.cloned.1.call-start = ((), (), s32[]{:S(2)}) async-start(), calls=%async_computation.6 | async-start | bytes 3538944 | tf_op jit(solution)/shard_map/reduce_scatter | solution.py:193
  334.9 5.8 %copy-start.1 = (bf16[4096,320]{1,0:T(8,128)(2,1)S(1)}, bf16[4096,320]{1,0:T(8,128)(2,1)}, u32[]{:S(2)}) copy-start(bf16[4096,320]{1,0:T(8,128)(2,1)} %all-gather.8.cloned.1.call-done) | copy-start | bytes 7864324
Sparse Core Ops, SparseCore 0:
  9.8 41.0 all-gather.3
  53.8 139.1 all-gather.5
  196.0 138.8 all-gather.7
  346.9 45.6 reduce-scatter.1
where the time goes:
time: 401 us; the launch traced here: 399 us
  waiting for transfers between devices  319 us (80%)
  starting transfers between devices  30.7 us (8%)
  matrix products  17.8 us (4%)
  between operations  14.2 us (4%)
  other arithmetic  9.83 us (2%)
  local copies, waits for them, and re-layouts  7.35 us (2%)
    all_gather x1, waiting for transfers between devices, sent_together(): out = lax.all_gather(both, axis, axis=dim, tiled=True)  142 us
    all_gather x1, waiting for transfers between devices, gather_turned(): out = lax.all_gather(both, axis, axis=0, tiled=True)  91.8 us
    reduce_scatter x1, waiting for transfers between devices, shards(): lax.psum_scatter((jnp.dot(conv_out, conv_full, preferred_element_type=jnp...  45.8 us
    all_gather x1, waiting for transfers between devices, shards(): lax.all_gather(normed, 'tp', axis=0, tiled=True)  34.7 us
    all_to_all x2, starting transfers between devices, sent_to_all(): lax.all_to_all(jnp.broadcast_to(value[None], (count, *value.shape)), axis...  25.7 us
  transfers between devices with their start and end apart: 8, of which 5 were waited for; matrix products, arithmetic and copies ran while one was open for 6% of the time, Pallas kernels for 0%

commit v1 on v0

v1 whole, which is shorter than its diff:
```python
import jax
import jax.numpy as jnp
from jax import lax
from jax.experimental import pallas as pl
from jax.experimental.pallas import tpu as pltpu
from jax.sharding import PartitionSpec as P

MESH = pl.DeviceIdType.MESH
CONV_WIDTH = 1024
RATE_SCALE = 8.0
NZ, NY, NX, NC = 16, 4, 4, 2
HALF = NZ // 2


def rem(a, n):
    return lax.rem(a + 4 * n, n)


class Gather:
    def __init__(self, a, b, rows, sems, pos):
        self.a, self.b, self.rows = a, b, rows
        self.s, self.r = sems[: len(sems) // 2], sems[len(sems) // 2 :]
        self.z, self.y = pos
        self.sent = []

    def at(self, ref, z, y):
        rows = self.rows
        return ref.at[pl.ds(pl.multiple_of((rem(z, NZ) * NY + rem(y, NY)) * rows, rows), rows)]

    def copy(self, ref, chunk, kind, index, to):
        block = self.at(ref, *chunk)
        return pltpu.make_async_remote_copy(
            src_ref=block,
            dst_ref=block,
            send_sem=self.s[kind].at[index],
            recv_sem=self.r[kind].at[index],
            device_id={"sp": rem(to[0], NZ) * NY + rem(to[1], NY)},
            device_id_type=MESH,
        )

    def send(self, *args):
        self.copy(*args).start()
        self.sent.append(args)

    def arrived(self, ref, chunk, kind, index):
        self.copy(ref, chunk, kind, index, (self.z + 1, self.y)).wait_recv()

    def start(self):
        z, y, a, b = self.z, self.y, self.a, self.b
        self.send(b, (z, y), 3, 0, (z + 1, y))
        self.send(b, (z, y), 4, 0, (z - 1, y))
        self.send(a, (z, y), 0, 0, (z, y + 1))
        self.send(a, (z, y), 0, 2, (z, y + 3))
        self.send(a, (z, y), 0, 1, (z, y + 2))
        self.send(a, (z, y), 1, 0, (z + 1, y))
        self.send(a, (z, y), 2, 0, (z - 1, y))
        self.spread(0)

    def start_y(self):
        z, y, a = self.z, self.y, self.a
        for d in (1, 3, 2):
            self.arrived(a, (z, y - d), 0, d - 1)
            self.send(a, (z, y - d), 1, d, (z + 1, y))
            self.send(a, (z, y - d), 2, d, (z - 1, y))

    def spread(self, k):
        z, y = self.z, self.y
        self.send(self.b, (z - k, y), 5, 3 * k, (z, y + 1))
        self.send(self.b, (z - k, y), 5, 3 * k + 1, (z, y - 1))

    def along_z(self, s):
        z, y, a, b = self.z, self.y, self.a, self.b
        self.arrived(b, (z - s, y), 3, s - 1)
        if s < HALF:
            self.send(b, (z - s, y), 3, s, (z + 1, y))
            self.arrived(b, (z + s, y), 4, s - 1)
            if s < HALF - 1:
                self.send(b, (z + s, y), 4, s, (z - 1, y))
            self.spread(s)
            self.spread(NZ - s)
        else:
            self.spread(s)
        for d in (0, 1, 3, 2):
            self.arrived(a, (z - s, y - d), 1, 4 * (s - 1) + d)
            if s < HALF:
                self.send(a, (z - s, y - d), 1, 4 * s + d, (z + 1, y))
                self.arrived(a, (z + s, y - d), 2, 4 * (s - 1) + d)
                if s < HALF - 1:
                    self.send(a, (z + s, y - d), 2, 4 * s + d, (z - 1, y))

    def along_y(self, k):
        z, y = self.z, self.y
        turn = 1 - 2 * (k % 2)
        self.arrived(self.b, (z - k, y - 1), 5, 3 * k)
        self.arrived(self.b, (z - k, y + 1), 5, 3 * k + 1)
        self.send(self.b, (z - k, y - turn), 5, 3 * k + 2, (z, y + turn))

    def along_y_last(self, k):
        self.arrived(self.b, (self.z - k, self.y + 2), 5, 3 * k + 2)

    def finish(self):
        for args in self.sent:
            self.copy(*args).wait_send()

    @staticmethod
    def semaphores():
        counts = [3, 4 * HALF, 4 * HALF, HALF, HALF, 3 * NZ]
        return [pltpu.SemaphoreType.DMA((n,)) for n in counts + counts]


N_SEMS = 12


def groups_of(step):
    if step == 0:
        return [0]
    if step < HALF:
        return [step, NZ - step]
    return [step] if step == HALF else []


def first_kernel(tokens, gain, wc_own, wr_own, oc_own, or_own, proj, oc, orr, *scratch):
    nt, wc, wr, acc_c, acc_r = scratch[:5]
    sems_in, sems_out = scratch[5 : 5 + N_SEMS], scratch[5 + N_SEMS : 5 + 2 * N_SEMS]
    tok_s, tok_r = scratch[5 + 2 * N_SEMS :]
    sp, tp = lax.axis_index("sp"), lax.axis_index("tp")
    z, y, x, c = sp // NY, sp % NY, tp // NC, tp % NC
    rows = wc_own.shape[0]
    n_tok = tokens.shape[0]
    width = tokens.shape[1]

    barrier = pltpu.get_barrier_semaphore()
    for dz, dy in ((1, 0), (-1, 0), (0, 1), (0, 2), (0, 3)):
        pl.semaphore_signal(
            barrier, inc=1, device_id={"sp": rem(z + dz, NZ) * NY + rem(y + dy, NY)}, device_id_type=MESH
        )
    for dx, dc in ((0, 1), (1, 0), (-1, 0)):
        pl.semaphore_signal(
            barrier, inc=1, device_id={"tp": rem(x + dx, NX) * NC + rem(c + dc, NC)}, device_id_type=MESH
        )

    own = pl.ds(pl.multiple_of(sp * rows, rows), rows)
    wc[own] = wc_own[...]
    wr[own] = wr_own[...]
    oc[own] = oc_own[...]
    orr[own] = or_own[...]
    pl.semaphore_wait(barrier, 8)

    g_in = Gather(wc, wr, rows, sems_in, (z, y))
    g_out = Gather(oc, orr, rows, sems_out, (z, y))
    g_in.start()

    def tok_at(xx, cc, lanes=None):
        r = pl.ds(pl.multiple_of((rem(xx, NX) * NC + rem(cc, NC)) * n_tok, 16), n_tok)
        return nt.at[r] if lanes is None else nt.at[r, lanes]

    def tok_copy(block, index, xx, cc):
        return pltpu.make_async_remote_copy(
            src_ref=block, dst_ref=block, send_sem=tok_s.at[index], recv_sem=tok_r.at[index],
            device_id={"tp": rem(xx, NX) * NC + rem(cc, NC)}, device_id_type=MESH,
        )

    t_sent = []

    def tok_send(*args):
        tok_copy(*args).start()
        t_sent.append(args)

    lo, hi = pl.ds(0, width // 2), pl.ds(width // 2, width // 2)

    widened = tokens[...].astype(jnp.float32)
    inverse = lax.rsqrt(jnp.mean(widened * widened, axis=-1, keepdims=True) + 1e-06)
    tok_at(x, c)[...] = (widened * inverse * gain[...]).astype(jnp.bfloat16)
    tok_send(tok_at(x, c), 0, x + 1, c)
    tok_send(tok_at(x, c), 1, x - 1, c)
    tok_send(tok_at(x, c), 4, x, c + 1)
    g_in.start_y()
    acc_c[...] = jnp.zeros_like(acc_c)
    acc_r[...] = jnp.zeros_like(acc_r)

    def tokens_forward():
        tok_copy(tok_at(x - 1, c), 0, x + 1, c).wait_recv()
        tok_send(tok_at(x - 1, c, lo), 2, x + 1, c)
        tok_send(tok_at(x - 1, c), 5, x, c + 1)
        tok_copy(tok_at(x + 1, c), 1, x + 1, c).wait_recv()
        tok_send(tok_at(x + 1, c, hi), 3, x - 1, c)
        tok_send(tok_at(x + 1, c), 6, x, c + 1)

    def tokens_last():
        tok_copy(tok_at(x + 2, c, lo), 2, x + 1, c).wait_recv()
        tok_send(tok_at(x + 2, c, lo), 7, x, c + 1)
        tok_copy(tok_at(x + 2, c, hi), 3, x + 1, c).wait_recv()
        tok_send(tok_at(x + 2, c, hi), 8, x, c + 1)
        tok_copy(tok_at(x, c + 1), 4, x + 1, c).wait_recv()
        tok_copy(tok_at(x - 1, c + 1), 5, x + 1, c).wait_recv()
        tok_copy(tok_at(x + 1, c + 1), 6, x + 1, c).wait_recv()
        tok_copy(tok_at(x + 2, c + 1, lo), 7, x + 1, c).wait_recv()
        tok_copy(tok_at(x + 2, c + 1, hi), 8, x + 1, c).wait_recv()

    def multiply(acc, w, first, count):
        def body(i, carry):
            cols = pl.ds(pl.multiple_of(rem(z - first - i, NZ) * (NY * rows), NY * rows), NY * rows)
            acc[...] += jnp.dot(nt[:, cols], w[cols, :], preferred_element_type=jnp.float32)
            return carry

        lax.fori_loop(0, count, body, 0)

    def multiply_runs(acc, w, steps):
        ks = sorted(k for s in steps for k in groups_of(s))
        runs = []
        for k in ks:
            if runs and runs[-1][0] + runs[-1][1] == k:
                runs[-1][1] += 1
            else:
                runs.append([k, 1])
        for first, count in runs:
            multiply(acc, w, first, count)

    go = 5
    for step in range(1, HALF + 3):
        if step == 2:
            g_out.start()
        if step <= HALF:
            g_in.along_z(step)
        if step == 3:
            g_out.start_y()
        if 2 < step:
            if step - 2 <= HALF:
                g_out.along_z(step - 2)
        for k in groups_of(step - 1):
            g_in.along_y(k)
        if step >= 2:
            for k in groups_of(step - 2):
                g_in.along_y_last(k)
        if step >= 4:
            for k in groups_of(step - 3):
                g_out.along_y(k)
        elif step == 3:
            g_out.along_y(0)
        if step == 3:
            tokens_forward()
        if step == go:
            tokens_last()
            multiply_runs(acc_c, wc, range(0, step + 1))
            multiply_runs(acc_r, wr, range(0, step - 1))
        elif step > go:
            multiply_runs(acc_c, wc, [step])
            multiply_runs(acc_r, wr, [step - 2])
    width_c = wc.shape[1]
    proj[:, :width_c] = acc_c[...].astype(jnp.bfloat16)
    proj[:, width_c:] = acc_r[...].astype(jnp.bfloat16)
    for k in groups_of(HALF):
        g_out.along_y(k)
    for k in range(NZ):
        g_out.along_y_last(k)
    g_in.finish()
    g_out.finish()
    for args in t_sent:
        tok_copy(*args).wait_send()


def passed_along(value, axis, by):
    count = lax.axis_size(axis)
    pairs = [(i, i + by) for i in range(count) if 0 <= i + by < count]
    return lax.ppermute(value, axis, pairs)


def sent_to_all(value, axis):
    count = lax.axis_size(axis)
    return lax.all_to_all(
        jnp.broadcast_to(value[None], (count, *value.shape)), axis, 0, 0, tiled=True
    )


def of_everyone(value, axis):
    return sent_to_all(value, axis).sum(axis=0)


def together(arrays, axis):
    ends = [0]
    for a in arrays:
        ends.append(ends[-1] + a.size)
    so_far = of_everyone(jnp.concatenate([a.ravel() for a in arrays]), axis)
    return tuple((so_far[b:e].reshape(a.shape) for a, b, e in zip(arrays, ends, ends[1:])))


def folded_in_pairs(pieces, combine):
    while len(jax.tree.leaves(pieces)[0]) > 1:
        pieces = jax.vmap(combine)(
            *(jax.tree.map(lambda part: part[side::2], pieces) for side in (0, 1))
        )
    return jax.tree.map(lambda part: part[0], pieces)


def carried_in(value, axis, combine, identity):
    count, mine = (lax.axis_size(axis), lax.axis_index(axis))
    passed = jnp.arange(count) < mine

    def kept(part, zero, own):
        return jnp.where(
            passed.reshape(-1, *(1 for _ in own.shape)), part, jnp.asarray(zero, own.dtype)
        )

    both = sent_to_all(jnp.stack(value), axis)
    pieces = (both[:, 0], both[:, 1])
    return folded_in_pairs(jax.tree.map(kept, pieces, identity, value), combine)


def causal_window(edge, current, weights):
    extended = jnp.concatenate([edge, current], axis=0).astype(jnp.float32)
    taps_wide = weights.astype(jnp.float32)
    length = current.shape[0]
    result = jnp.zeros((length, current.shape[1]), jnp.float32)
    for lag_index in range(weights.shape[0]):
        result = result + taps_wide[lag_index][None, :] * extended[lag_index : lag_index + length]
    return result


def chain_step(earlier, latter):
    return (earlier[0] * latter[0], latter[0] * earlier[1] + latter[1])


def glu_of(conv_val, conv_gate):
    return (conv_val.astype(jnp.float32) * jax.nn.sigmoid(conv_gate.astype(jnp.float32))).astype(
        jnp.bfloat16
    )


def shards(
    tokens, norm_gain, conv_val_w, conv_gate_w, rec_gate_w, rec_in_w, conv_taps, conv_bias, conv_gain,
    short_taps, decay_map, input_map, decay_base, decay_jump, out_conv_w, out_rec_w,
):
    conv_cols = conv_val_w.shape[1]
    rec_cols = rec_in_w.shape[1]
    conv_lags = conv_taps.shape[0] - 1
    short_lags = short_taps.shape[0] - 1
    n_tp, n_sp = lax.axis_size("tp"), lax.axis_size("sp")
    n_tok, width = tokens.shape
    rec_pad = -rec_cols % 128
    vmem = pl.BlockSpec(memory_space=pltpu.VMEM)
    projected, conv_full, rec_full = pl.pallas_call(
        first_kernel,
        out_shape=(
            jax.ShapeDtypeStruct((n_tok * n_tp, 2 * conv_cols + 2 * rec_cols), jnp.bfloat16),
            jax.ShapeDtypeStruct((width, conv_cols), jnp.bfloat16),
            jax.ShapeDtypeStruct((width, rec_cols + rec_pad), jnp.bfloat16),
        ),
        in_specs=[vmem] * 6,
        out_specs=(vmem,) * 3,
        scratch_shapes=[
            pltpu.VMEM((n_tok * n_tp, width), jnp.bfloat16),
            pltpu.VMEM((width, 2 * conv_cols), jnp.bfloat16),
            pltpu.VMEM((width, 2 * rec_cols), jnp.bfloat16),
            pltpu.VMEM((n_tok * n_tp, 2 * conv_cols), jnp.float32),
            pltpu.VMEM((n_tok * n_tp, 2 * rec_cols), jnp.float32),
            *Gather.semaphores(),
            *Gather.semaphores(),
            pltpu.SemaphoreType.DMA((9,)),
            pltpu.SemaphoreType.DMA((9,)),
        ],
        compiler_params=pltpu.CompilerParams(
            collective_id=0, has_side_effects=True, vmem_limit_bytes=60 * 1024 * 1024
        ),
    )(
        tokens,
        norm_gain[None, :],
        jnp.concatenate([conv_val_w, conv_gate_w], axis=1),
        jnp.concatenate([rec_gate_w, rec_in_w], axis=1),
        out_conv_w.T,
        jnp.pad(out_rec_w.T, ((0, 0), (0, rec_pad))),
    )
    glu = glu_of(projected[:, :conv_cols], projected[:, conv_cols : 2 * conv_cols])
    rec_gate = projected[:, 2 * conv_cols : 2 * conv_cols + rec_cols]
    rec_in = projected[:, 2 * conv_cols + rec_cols :]
    conv_edge, rec_edge = passed_along((glu[-conv_lags:], rec_in[-short_lags:]), "sp", 1)
    filtered = causal_window(conv_edge, glu, conv_taps) + conv_bias[None, :]
    row_total, row_squares = together(
        (jnp.sum(filtered, axis=1), jnp.sum(filtered * filtered, axis=1)), "tp"
    )
    row_mean = row_total / CONV_WIDTH
    spread = row_squares / CONV_WIDTH - row_mean * row_mean
    centered = filtered - row_mean[:, None]
    conv_out = jax.nn.silu(centered * lax.rsqrt(spread + 1e-05)[:, None] * conv_gain).astype(
        jnp.bfloat16
    )
    smoothed = causal_window(rec_edge, rec_in, short_taps).astype(jnp.bfloat16)
    length = smoothed.shape[0]
    grouped = smoothed.reshape(length, decay_map.shape[0], decay_map.shape[1])
    retain = jax.nn.sigmoid(
        jnp.einsum("thi,hio->tho", grouped, decay_map, preferred_element_type=jnp.float32).reshape(
            length, rec_cols
        )
    )
    admit = jax.nn.sigmoid(
        jnp.einsum("thi,hio->tho", grouped, input_map, preferred_element_type=jnp.float32).reshape(
            length, rec_cols
        )
    )
    log_decay = -RATE_SCALE * retain * jax.nn.softplus(-decay_base)[None, :] + decay_jump
    decay = jnp.exp(log_decay)
    inflow = jnp.sqrt(-jnp.expm1(2.0 * log_decay)) * admit * smoothed.astype(jnp.float32)
    products, local_state = lax.associative_scan(chain_step, (decay, inflow), axis=0)
    entering = carried_in(
        (products[-1], local_state[-1]),
        "sp",
        chain_step,
        (jnp.ones((rec_cols,), jnp.float32), jnp.zeros((rec_cols,), jnp.float32)),
    )
    state = local_state + products * entering[1][None, :]
    rec_out = (jax.nn.gelu(rec_gate.astype(jnp.float32)) * state).astype(jnp.bfloat16)
    nt_dims = (((1,), (1,)), ((), ()))
    return lax.psum_scatter(
        (
            lax.dot_general(conv_out, conv_full, nt_dims, preferred_element_type=jnp.float32)
            + lax.dot_general(
                rec_out, rec_full[:, :rec_cols], nt_dims, preferred_element_type=jnp.float32
            )
        ).astype(jnp.bfloat16),
        "tp",
        scatter_dimension=0,
        tiled=True,
    )


def solution(mesh):
    in_specs = (
        P(("sp", "tp"), None), P(), P("sp", "tp"), P("sp", "tp"), P("sp", "tp"), P("sp", "tp"),
        P(None, "tp"), P("tp"), P("tp"), P(None, "tp"), P("tp", None, None), P("tp", None, None),
        P("tp"), P("sp", "tp"), P("tp", "sp"), P("tp", "sp"),
    )
    return jax.shard_map(
        shards, mesh=mesh, in_specs=in_specs, out_specs=P(("sp", "tp"), None), check_vma=False
    )
```

time: 401 us -> 198 us (0.49)
  waiting for transfers between devices: 319 us -> 47 us
  Pallas kernels: 0 us -> 84.2 us
  starting transfers between devices: 30.7 us -> 20.4 us
  matrix products: 17.8 us -> 11.4 us
    all_gather x3 -> x0, waiting for transfers between devices: 269 us -> none  [the longest x1 142 us: sent_together(): out = lax.all_gather(both, axis, axis=dim, tiled=True)]
    pallas_call x0 -> x1, Pallas kernels: none -> 84.2 us  [shards(): pl.pallas_call(first_kernel, out_shape=(jax.ShapeDtypeStruct((n_tok * n_t...]
    reduce_scatter x1, waiting for transfers between devices: 45.8 us -> 32.6 us  [shards(): lax.psum_scatter((lax.dot_general(conv_out, conv_full, nt_dims, preferred...]
    all_to_all x2, starting transfers between devices: 25.7 us -> 15.6 us  [sent_to_all(): lax.all_to_all(jnp.broadcast_to(value[None], (count, *value.shape)), axis...]
    all_to_all x2, waiting for transfers between devices: 4.68 us -> 14.3 us  [sent_to_all(): lax.all_to_all(jnp.broadcast_to(value[None], (count, *value.shape)), axis...]
    dot_general x3 -> x2, matrix products: 17.2 us -> 10.9 us  [the longest x1 5.84 us: shards(): lax.dot_general(rec_out, rec_full[:, :rec_cols], nt_dims, preferred_eleme...]
  transfers between devices with their start and end apart: 8 -> 5, of which waited for: 5 -> 3; matrix products, arithmetic and copies ran while one was open for 6% -> 8% of each run, Pallas kernels for 0% -> 0%
where the time goes in v1:
time: 198 us; the launch traced here: 196 us
  Pallas kernels  84.2 us (43%)
  waiting for transfers between devices  47 us (24%)
  starting transfers between devices  20.4 us (10%)
  between operations  14.4 us (7%)
  matrix products  11.4 us (6%)
  local copies, waits for them, and re-layouts  11.3 us (6%)
  other arithmetic  7.58 us (4%)
    pallas_call x1, Pallas kernels, shards(): pl.pallas_call(first_kernel, out_shape=(jax.ShapeDtypeStruct((n_tok * n_t...  84.2 us
    reduce_scatter x1, waiting for transfers between devices, shards(): lax.psum_scatter((lax.dot_general(conv_out, conv_full, nt_dims, preferred...  32.6 us
    all_to_all x2, starting transfers between devices, sent_to_all(): lax.all_to_all(jnp.broadcast_to(value[None], (count, *value.shape)), axis...  15.6 us
    all_to_all x2, waiting for transfers between devices, sent_to_all(): lax.all_to_all(jnp.broadcast_to(value[None], (count, *value.shape)), axis...  14.3 us
    dot_general x1, matrix products, shards(): lax.dot_general(rec_out, rec_full[:, :rec_cols], nt_dims, preferred_eleme...  5.84 us
    dot_general x1, matrix products, shards(): lax.dot_general(conv_out, conv_full, nt_dims, preferred_element_type=jnp....  5.05 us
    ppermute x2, starting transfers between devices, passed_along(): return lax.ppermute(value, axis, pairs)  4.58 us
  transfers between devices with their start and end apart: 5, of which 3 were waited for; matrix products, arithmetic and copies ran while one was open for 8% of the time, Pallas kernels for 0%

profile of v1, /device:TPU:1, one launch (start us, length us, event | category | flops | bytes accessed | tf_op | source)
XLA Modules:
  0.0 196.3 jit_solution(13171934848322666208)
XLA Ops:
  6.5 1.4 pad_maximum_fusion.7.wc_own
  7.9 1.4 pad.102.or_own
  9.3 1.5 pad_maximum_fusion.4.wr_own
  10.7 84.2 %shard_map.154 = (bf16[384,640]{1,0:T(8,128)(2,1)}, bf16[4096,128]{1,0:T(8,128)(2,1)}, bf16[4096,256]{1,0:T(8,128)(2,1)}) custom-call(bf16[48,4096]{1,0:T(8,128)(2,1)} %tokens.1, f32[1,4096]{1,0:T(1,128)} %bitcast.93, bf16[64,256]{1,0:T(8,128)(2,1)} %pad_maximum_fusion.7.wc_own, bf16[64,384]{1,0:T(8,128)(2,1)} %pad_maximum_fusion.4.wr_own, ...), custom_call_target="tpu_custom_call" | custom-call | tf_op jit(solution)/shard_map/pallas_call | solution.py:341
  94.9 0.8 slice.627
  95.7 2.7 %collective-permute-start.1 = (bf16[3,192]{1,0:T(4,128)(2,1)S(1)}, bf16[3,192]{1,0:T(4,128)(2,1)S(1)}, u32[]{:S(2)}, u32[]{:S(2)}) collective-permute-start(bf16[3,192]{1,0:T(4,128)(2,1)S(1)} %slice.627), channel_id=1, source_target_pairs={{0,8},{8,16},{16,24},{24,32},{32,40},{40,48},{48,56},{56,64},{64,7... | collective-permute-start | bytes 3464 | tf_op jit(solution)/shard_map/ppermute | solution.py:265
  98.4 1.0 multiply_convert_fusion.1
  99.4 1.9 collective-permute-start
  101.3 0.7 convert_element_type.41
  102.1 0.7 fusion.74
  102.7 0.8 fusion.87
  103.6 1.0 slice.628
  104.7 1.1 copy.48
  105.9 0.2 fusion.15
  106.0 0.1 copy.45
  106.2 0.3 fusion.3
  106.5 0.2 copy.50
  106.7 0.3 fusion.6
  106.9 0.2 copy.47
  107.1 0.5 convert_multiply_fusion.3
  107.6 0.3 slice.696
  107.9 0.2 slice.640
  108.1 0.2 slice.639
  108.3 0.2 slice.642
  108.4 0.2 slice.638
  108.6 0.3 slice.637
  108.9 0.1 multiply_add_fusion.1
  109.0 0.1 slice.694
  109.3 0.1 slice.643
  111.4 0.1 fusion.19
  111.5 0.1 pad.133
  111.6 0.1 pad.117
  111.6 0.1 pad.118
  111.7 0.1 pad.134
  111.8 0.1 copy-done.4
  111.9 0.8 fusion.80
  112.7 0.6 broadcast_in_dim.41
  113.3 4.8 %all-to-all-start = ((f32[8,1,768]{2,1,0:T(1,128)}), f32[8,1,768]{2,1,0:T(1,128)S(1)}, u32[]{:S(2)}, u32[]{:S(2)}) async-start(f32[8,1,768]{2,1,0:T(1,128)} %broadcast_in_dim.41), calls=%async_computation | async-start | bytes 49152 | tf_op jit(solution)/shard_map/all_to_all | solution.py:270
  118.1 4.7 %all-to-all-done = f32[8,1,768]{2,1,0:T(1,128)S(1)} async-done(((f32[8,1,768]{2,1,0:T(1,128)}), f32[8,1,768]{2,1,0:T(1,128)S(1)}, u32[]{:S(2)}, u32[]{:S(2)}) %all-to-all-start) | async-done | bytes 24608 | tf_op jit(solution)/shard_map/all_to_all | solution.py:270
  122.8 0.7 broadcast_in_dim.43
  123.5 10.8 %all-to-all-start.1 = ((f32[64,2,192]{2,1,0:T(2,128)}), f32[64,2,192]{2,1,0:T(2,128)}, u32[]{:S(2)}, u32[]{:S(2)}) async-start(f32[64,2,192]{2,1,0:T(2,128)} %broadcast_in_dim.43), calls=%async_computation.1 | async-start | bytes 262144 | tf_op jit(solution)/shard_map/all_to_all | solution.py:270
  134.3 0.2 reduce-scatter.2.cloned.1.call-start
  134.6 5.1 %fusion.58 = f32[384,4096]{1,0:T(8,128)} fusion(bf16[4096,128]{1,0:T(8,128)(2,1)} %get-tuple-element.9, f32[384,128]{1,0:T(8,128)S(1)} %get-tuple-element.17, f32[128]{0:T(128)S(1)} %copy-done.3, f32[384]{0:T(512)S(1)} %get-tuple-element.92, f32[384]{0:T(512)S(1)} %get-tuple-element.91), kind=kOutput, calls=%fused_computation.111 | convolution fusion | flops 403046400 | bytes 7540224 | tf_op jit(solution)/shard_map/dot_general | solution.py:414
  139.7 9.6 %all-to-all-done.1 = f32[64,2,192]{2,1,0:T(2,128)} async-done(((f32[64,2,192]{2,1,0:T(2,128)}), f32[64,2,192]{2,1,0:T(2,128)}, u32[]{:S(2)}, u32[]{:S(2)}) %all-to-all-start.1) | async-done | bytes 98336 | tf_op jit(solution)/shard_map/all_to_all | solution.py:270
  149.3 1.1 fusion.82
  150.4 0.1 fusion.64
  151.0 5.8 %add_convert_fusion = bf16[384,4096]{1,0:T(8,128)(2,1)} fusion(f32[384,4096]{1,0:T(8,128)} %fusion.58, bf16[4096,256]{1,0:T(8,128)(2,1)S(1)} %copy-done.1, f32[384,192]{1,0:T(8,128)S(1)} %pad.133, f32[384,192]{1,0:T(8,128)} %copy-done.2, f32[384,192]{1,0:T(8,128)S(1)} %pad.117, f32[384,192]{1,0:T(8,128)S(1)} %pad.118, f32[192]{0:T(256)S(1)} %bitcast.103, ...), kind=kOutput, calls=%fused_computation | convolution fusion | flops 608231424 | bytes 13009664 | tf_op jit(solution)/shard_map/dot_general | solution.py:415
  156.8 32.6 %reduce-scatter.2.cloned.1.call-done = bf16[48,4096]{1,0:T(8,128)(2,1)} async-done(((bf16[384,4096]{1,0:T(8,128)(2,1)}), bf16[48,4096]{1,0:T(8,128)(2,1)}) %reduce-scatter.2.cloned.1.call-update) | async-done | bytes 393232 | tf_op jit(solution)/shard_map/reduce_scatter | solution.py:412
  (167 shorter events, 2.4 us)
Async XLA Ops:
  6.5 99.6 %copy-start = (bf16[3,64,64]{2,1,0:T(8,128)(2,1)S(1)}, bf16[3,64,64]{2,1,0:T(8,128)(2,1)}, u32[]{:S(2)}) copy-start(bf16[3,64,64]{2,1,0:T(8,128)(2,1)} %param.27) | copy-start | bytes 73732
  94.9 11.7 %copy-start.5 = (bf16[3,64,64]{2,1,0:T(8,128)(2,1)S(1)}, bf16[3,64,64]{2,1,0:T(8,128)(2,1)}, u32[]{:S(2)}) copy-start(bf16[3,64,64]{2,1,0:T(8,128)(2,1)} %param.26) | copy-start | bytes 73732
  95.7 10.1 %collective-permute-start.1 = (bf16[3,192]{1,0:T(4,128)(2,1)S(1)}, bf16[3,192]{1,0:T(4,128)(2,1)S(1)}, u32[]{:S(2)}, u32[]{:S(2)}) collective-permute-start(bf16[3,192]{1,0:T(4,128)(2,1)S(1)} %slice.627), channel_id=1, source_target_pairs={{0,8},{8,16},{16,24},{24,32},{32,40},{40,48},{48,56},{56,64},{64,7... | collective-permute-start | bytes 3464 | tf_op jit(solution)/shard_map/ppermute | solution.py:265
  99.4 12.4 %collective-permute-start = (bf16[30,128]{1,0:T(8,128)(2,1)S(1)}, bf16[30,128]{1,0:T(8,128)(2,1)S(1)}, u32[]{:S(2)}, u32[]{:S(2)}) collective-permute-start(bf16[30,128]{1,0:T(8,128)(2,1)S(1)} %slice.741), channel_id=1, source_target_pairs={{0,8},{8,16},{16,24},{24,32},{32,40},{40,48},{48,56},{56,64},{64,7... | collective-permute-start | bytes 23048 | tf_op jit(solution)/shard_map/ppermute | solution.py:265
  111.3 0.7 copy-start.4
  111.8 0.9 copy-start.2
  111.9 22.6 %copy-start.3 = (f32[128]{0:T(128)S(1)}, f32[128]{0:T(128)}, u32[]{:S(2)}) copy-start(f32[128]{0:T(128)} %param.24) | copy-start | bytes 1540
  113.3 9.5 %all-to-all-start = ((f32[8,1,768]{2,1,0:T(1,128)}), f32[8,1,768]{2,1,0:T(1,128)S(1)}, u32[]{:S(2)}, u32[]{:S(2)}) async-start(f32[8,1,768]{2,1,0:T(1,128)} %broadcast_in_dim.41), calls=%async_computation | async-start | bytes 49152 | tf_op jit(solution)/shard_map/all_to_all | solution.py:270
  123.5 25.8 %all-to-all-start.1 = ((f32[64,2,192]{2,1,0:T(2,128)}), f32[64,2,192]{2,1,0:T(2,128)}, u32[]{:S(2)}, u32[]{:S(2)}) async-start(f32[64,2,192]{2,1,0:T(2,128)} %broadcast_in_dim.43), calls=%async_computation.1 | async-start | bytes 262144 | tf_op jit(solution)/shard_map/all_to_all | solution.py:270
  134.3 55.2 %reduce-scatter.2.cloned.1.call-start = ((), (), s32[]{:S(2)}) async-start(), calls=%async_computation.3 | async-start | bytes 3538944 | tf_op jit(solution)/shard_map/reduce_scatter | solution.py:412
  134.6 16.4 %copy-start.1 = (bf16[4096,256]{1,0:T(8,128)(2,1)S(1)}, bf16[4096,256]{1,0:T(8,128)(2,1)}, u32[]{:S(2)}) copy-start(bf16[4096,256]{1,0:T(8,128)(2,1)} %get-tuple-element.10) | copy-start | bytes 6291460
Sparse Core Ops, SparseCore 0:
  157.0 32.4 reduce-scatter.1

commit v2 on v1

v2 whole, which is shorter than its diff:
```python
import jax
import jax.numpy as jnp
from jax import lax
from jax.experimental import pallas as pl
from jax.experimental.pallas import tpu as pltpu
from jax.sharding import PartitionSpec as P

MESH = pl.DeviceIdType.MESH
CONV_WIDTH = 1024
RATE_SCALE = 8.0
NZ, NY, NX, NC = 16, 4, 4, 2
HALF = NZ // 2


def rem(a, n):
    return lax.rem(a + 4 * n, n)


class Gather:
    def __init__(self, a, b, rows, sems, pos):
        self.a, self.b, self.rows = a, b, rows
        self.s, self.r = sems[: len(sems) // 2], sems[len(sems) // 2 :]
        self.z, self.y = pos
        self.sent = []

    def at(self, ref, z, y):
        rows = self.rows
        return ref.at[pl.ds(pl.multiple_of((rem(z, NZ) * NY + rem(y, NY)) * rows, rows), rows)]

    def copy(self, ref, chunk, kind, index, to):
        block = self.at(ref, *chunk)
        return pltpu.make_async_remote_copy(
            src_ref=block,
            dst_ref=block,
            send_sem=self.s[kind].at[index],
            recv_sem=self.r[kind].at[index],
            device_id={"sp": rem(to[0], NZ) * NY + rem(to[1], NY)},
            device_id_type=MESH,
        )

    def send(self, *args):
        self.copy(*args).start()
        self.sent.append(args)

    def arrived(self, ref, chunk, kind, index):
        self.copy(ref, chunk, kind, index, (self.z + 1, self.y)).wait_recv()

    def start(self):
        z, y, a, b = self.z, self.y, self.a, self.b
        self.send(b, (z, y), 3, 0, (z + 1, y))
        self.send(b, (z, y), 4, 0, (z - 1, y))
        self.send(a, (z, y), 0, 0, (z, y + 1))
        self.send(a, (z, y), 0, 2, (z, y + 3))
        self.send(a, (z, y), 0, 1, (z, y + 2))
        self.send(a, (z, y), 1, 0, (z + 1, y))
        self.send(a, (z, y), 2, 0, (z - 1, y))
        self.spread(0)

    def start_y(self):
        z, y, a = self.z, self.y, self.a
        for d in (1, 3, 2):
            self.arrived(a, (z, y - d), 0, d - 1)
            self.send(a, (z, y - d), 1, d, (z + 1, y))
            self.send(a, (z, y - d), 2, d, (z - 1, y))

    def spread(self, k):
        z, y = self.z, self.y
        self.send(self.b, (z - k, y), 5, 3 * k, (z, y + 1))
        self.send(self.b, (z - k, y), 5, 3 * k + 1, (z, y - 1))

    def along_z(self, s):
        z, y, a, b = self.z, self.y, self.a, self.b
        self.arrived(b, (z - s, y), 3, s - 1)
        if s < HALF:
            self.send(b, (z - s, y), 3, s, (z + 1, y))
            self.arrived(b, (z + s, y), 4, s - 1)
            if s < HALF - 1:
                self.send(b, (z + s, y), 4, s, (z - 1, y))
            self.spread(s)
            self.spread(NZ - s)
        else:
            self.spread(s)
        for d in (0, 1, 3, 2):
            self.arrived(a, (z - s, y - d), 1, 4 * (s - 1) + d)
            if s < HALF:
                self.send(a, (z - s, y - d), 1, 4 * s + d, (z + 1, y))
                self.arrived(a, (z + s, y - d), 2, 4 * (s - 1) + d)
                if s < HALF - 1:
                    self.send(a, (z + s, y - d), 2, 4 * s + d, (z - 1, y))

    def along_y(self, k):
        z, y = self.z, self.y
        turn = 1 - 2 * (k % 2)
        self.arrived(self.b, (z - k, y - 1), 5, 3 * k)
        self.arrived(self.b, (z - k, y + 1), 5, 3 * k + 1)
        self.send(self.b, (z - k, y - turn), 5, 3 * k + 2, (z, y + turn))

    def along_y_last(self, k):
        self.arrived(self.b, (self.z - k, self.y + 2), 5, 3 * k + 2)

    def finish(self):
        for args in self.sent:
            self.copy(*args).wait_send()

    @staticmethod
    def semaphores():
        counts = [3, 4 * HALF, 4 * HALF, HALF, HALF, 3 * NZ]
        return [pltpu.SemaphoreType.DMA((n,)) for n in counts + counts]


N_SEMS = 12


def groups_of(step):
    if step == 0:
        return [0]
    if step < HALF:
        return [step, NZ - step]
    return [step] if step == HALF else []


def expm1_negated(v):
    series = jnp.ones_like(v)
    for n in range(9, 1, -1):
        series = 1.0 + series * v * (1.0 / n)
    return jnp.where(v > -0.5, -v * series, 1.0 - jnp.exp(v))


def softplus_negated(b):
    e = jnp.exp(-jnp.abs(b))
    w = e / (2.0 + e)
    q = w * w
    series = jnp.full_like(w, 1.0 / 15.0)
    for n in (13, 11, 9, 7, 5, 3, 1):
        series = 1.0 / n + series * q
    return jnp.maximum(-b, 0.0) + 2.0 * w * series


NT_DIMS = (((1,), (1,)), ((), ()))
TN_DIMS = (((0,), (0,)), ((), ()))
SEGS = 8


def whole_kernel(
    tokens, gain, wc_own, wr_own, oc_own, or_own, taps, bias, cgain, staps, dmap, imap, base, jump, out, *scratch
):
    (nt, wc, wr, acc_c, acc_r, oc, orr, ext_c, ext_r, filt, md, mi, stats, dbuf, ibuf, gbuf, co, ro,
     seg_e, cy, cz, pc, ps, pr, s2, sp_buf, sm_buf, two, from_m, from_p) = scratch[:30]
    scratch = scratch[30:]
    sems_in, sems_out = scratch[:N_SEMS], scratch[N_SEMS : 2 * N_SEMS]
    (tok_s, tok_r, edge_s, edge_r, stat_s, stat_r, cy_s, cy_r, cz_s, cz_r, pr_s, pr_r, x_s, x_r) = scratch[2 * N_SEMS :]
    sp, tp = lax.axis_index("sp"), lax.axis_index("tp")
    z, y, x, c = sp // NY, sp % NY, tp // NC, tp % NC
    rows = wc_own.shape[0]
    n_tok, width = tokens.shape
    length = acc_c.shape[0]
    cw = acc_c.shape[1] // 2
    rw = acc_r.shape[1] // 2
    f32, bf16 = jnp.float32, jnp.bfloat16

    barrier = pltpu.get_barrier_semaphore()
    for dz, dy in ((1, 0), (-1, 0), (0, 1), (0, 2), (0, 3)):
        pl.semaphore_signal(
            barrier, inc=1, device_id={"sp": rem(z + dz, NZ) * NY + rem(y + dy, NY)}, device_id_type=MESH
        )
    for d in (1, -1):
        pl.semaphore_signal(barrier, inc=1, device_id={"sp": rem(sp + d, NZ * NY)}, device_id_type=MESH)
    for d in range(1, NX * NC):
        pl.semaphore_signal(barrier, inc=1, device_id={"tp": rem(tp + d, NX * NC)}, device_id_type=MESH)

    own = pl.ds(pl.multiple_of(sp * rows, rows), rows)
    wc[own] = wc_own[...]
    wr[own] = wr_own[...]
    oc[own] = oc_own[...]
    orr[own] = or_own[...]
    pl.semaphore_wait(barrier, 7 + NX * NC - 1)

    g_in = Gather(wc, wr, rows, sems_in, (z, y))
    g_out = Gather(oc, orr, rows, sems_out, (z, y))
    g_in.start()

    def tok_rows(xx, cc):
        return pl.ds(pl.multiple_of((rem(xx, NX) * NC + rem(cc, NC)) * n_tok, 16), n_tok)

    def tok_at(xx, cc, lanes=None):
        r = tok_rows(xx, cc)
        return nt.at[r] if lanes is None else nt.at[r, lanes]

    def tok_copy(block, index, xx, cc):
        return pltpu.make_async_remote_copy(
            src_ref=block, dst_ref=block, send_sem=tok_s.at[index], recv_sem=tok_r.at[index],
            device_id={"tp": rem(xx, NX) * NC + rem(cc, NC)}, device_id_type=MESH,
        )

    t_sent = []

    def tok_send(*args):
        tok_copy(*args).start()
        t_sent.append(args)

    lo, hi = pl.ds(0, width // 2), pl.ds(width // 2, width // 2)

    widened = tokens[...].astype(f32)
    inverse = lax.rsqrt(jnp.mean(widened * widened, axis=-1, keepdims=True) + 1e-06)
    tok_at(x, c)[...] = (widened * inverse * gain[...]).astype(bf16)
    tok_send(tok_at(x, c), 0, x + 1, c)
    tok_send(tok_at(x, c), 1, x - 1, c)
    tok_send(tok_at(x, c), 4, x, c + 1)
    g_in.start_y()
    acc_c[...] = jnp.zeros_like(acc_c)
    acc_r[...] = jnp.zeros_like(acc_r)
    cy[...] = jnp.zeros_like(cy)
    cz[...] = jnp.zeros_like(cz)
    head = dmap.shape[1]
    for m, given in ((md, dmap), (mi, imap)):
        m[...] = jnp.zeros_like(m)
        for h in range(dmap.shape[0]):
            m[h * head : (h + 1) * head, h * head : (h + 1) * head] = given[h]

    def tokens_forward():
        tok_copy(tok_at(x - 1, c), 0, x + 1, c).wait_recv()
        tok_send(tok_at(x - 1, c, lo), 2, x + 1, c)
        tok_send(tok_at(x - 1, c), 5, x, c + 1)
        tok_copy(tok_at(x + 1, c), 1, x + 1, c).wait_recv()
        tok_send(tok_at(x + 1, c, hi), 3, x - 1, c)
        tok_send(tok_at(x + 1, c), 6, x, c + 1)

    def tokens_last():
        tok_copy(tok_at(x + 2, c, lo), 2, x + 1, c).wait_recv()
        tok_send(tok_at(x + 2, c, lo), 7, x, c + 1)
        tok_copy(tok_at(x + 2, c, hi), 3, x + 1, c).wait_recv()
        tok_send(tok_at(x + 2, c, hi), 8, x, c + 1)
        tok_copy(tok_at(x, c + 1), 4, x + 1, c).wait_recv()
        tok_copy(tok_at(x - 1, c + 1), 5, x + 1, c).wait_recv()
        tok_copy(tok_at(x + 1, c + 1), 6, x + 1, c).wait_recv()
        tok_copy(tok_at(x + 2, c + 1, lo), 7, x + 1, c).wait_recv()
        tok_copy(tok_at(x + 2, c + 1, hi), 8, x + 1, c).wait_recv()

    def multiply(acc, w, first, count):
        def body(i, carry):
            cols = pl.ds(pl.multiple_of(rem(z - first - i, NZ) * (NY * rows), NY * rows), NY * rows)
            acc[...] += jnp.dot(nt[:, cols], w[cols, :], preferred_element_type=f32)
            return carry

        lax.fori_loop(0, count, body, 0)

    def multiply_runs(acc, w, steps):
        ks = sorted(k for s in steps for k in groups_of(s))
        runs = []
        for k in ks:
            if runs and runs[-1][0] + runs[-1][1] == k:
                runs[-1][1] += 1
            else:
                runs.append([k, 1])
        for first, count in runs:
            multiply(acc, w, first, count)

    go = 5
    for step in range(1, HALF + 3):
        if step == 2:
            g_out.start()
        if step <= HALF:
            g_in.along_z(step)
        if step == 3:
            g_out.start_y()
        if 2 < step:
            if step - 2 <= HALF:
                g_out.along_z(step - 2)
        for k in groups_of(step - 1):
            g_in.along_y(k)
        if step >= 2:
            for k in groups_of(step - 2):
                g_in.along_y_last(k)
        if step >= 4:
            for k in groups_of(step - 3):
                g_out.along_y(k)
        elif step == 3:
            g_out.along_y(0)
        if step == 3:
            tokens_forward()
        if step == go:
            tokens_last()
            multiply_runs(acc_c, wc, range(0, step + 1))
            multiply_runs(acc_r, wr, range(0, step - 1))
        elif step > go:
            multiply_runs(acc_c, wc, [step])
            multiply_runs(acc_r, wr, [step - 2])

    c_pad, r_pad = ext_c.shape[0] - length, ext_r.shape[0] - length
    projected = acc_r[...].astype(bf16).astype(f32)
    ext_r[r_pad:, :] = projected[:, :rw]
    gate = projected[:, rw:]
    conv_val = acc_c[:, :cw].astype(bf16).astype(f32)
    conv_gate = acc_c[:, cw:].astype(bf16).astype(f32)
    ext_c[c_pad:, :] = (conv_val * jax.nn.sigmoid(conv_gate)).astype(bf16).astype(f32)

    def edge_copy(ref, pad, index):
        return pltpu.make_async_remote_copy(
            src_ref=ref.at[pl.ds(length, pad)], dst_ref=ref.at[pl.ds(0, pad)],
            send_sem=edge_s.at[index], recv_sem=edge_r.at[index],
            device_id={"sp": rem(sp + 1, NZ * NY)}, device_id_type=MESH,
        )

    edges = [edge_copy(ext_r, r_pad, 0), edge_copy(ext_c, c_pad, 1)]
    for e in edges:
        e.start()
    for k in groups_of(HALF):
        g_out.along_y(k)
    gbuf[...] = 0.5 * gate * (1.0 + jnp.tanh(0.7978845608028654 * (gate + 0.044715 * gate * gate * gate)))

    n_taps = taps.shape[0]
    wide = taps[...].astype(f32)
    tap_rows = 32

    def filter_rows(first):
        total = jnp.broadcast_to(bias[...], (tap_rows, cw))
        for k in range(n_taps):
            at = first + c_pad - (n_taps - 1) + k
            total = total + wide[k : k + 1, :] * ext_c[at : at + tap_rows, :]
        filt[first : first + tap_rows, :] = total

    for i in range(1, length // tap_rows):
        filter_rows(i * tap_rows)
    for e in edges:
        e.wait_recv()
    has = sp > 0
    ext_r[:r_pad, :] = jnp.where(has, ext_r[:r_pad, :], 0.0)
    ext_c[:c_pad, :] = jnp.where(has, ext_c[:c_pad, :], 0.0)
    filter_rows(0)

    filtered = filt[...]
    row_id = lax.broadcasted_iota(jnp.int32, (8, cw), 0)
    first_half = jnp.where(row_id < 4, 1.0, 0.0)
    exact = lax.Precision.HIGHEST
    stats[tp] = lax.dot_general(
        first_half, filtered, NT_DIMS, precision=exact, preferred_element_type=f32
    ) + lax.dot_general(
        1.0 - first_half, filtered * filtered, NT_DIMS, precision=exact, preferred_element_type=f32
    )

    def stat_copy(d):
        return pltpu.make_async_remote_copy(
            src_ref=stats.at[tp], dst_ref=stats.at[tp], send_sem=stat_s.at[d - 1], recv_sem=stat_r.at[d - 1],
            device_id={"tp": rem(tp + d, NX * NC)}, device_id_type=MESH,
        )

    def stat_arrival(d):
        slot = stats.at[rem(tp - d, NX * NC)]
        return pltpu.make_async_remote_copy(
            src_ref=slot, dst_ref=slot, send_sem=stat_s.at[d - 1], recv_sem=stat_r.at[d - 1],
            device_id={"tp": rem(tp + d, NX * NC)}, device_id_type=MESH,
        )

    for d in range(1, NX * NC):
        stat_copy(d).start()

    n_short = staps.shape[0]
    short = staps[...].astype(f32)
    smoothed = jnp.zeros((length, rw), f32)
    for k in range(n_short):
        at = r_pad - (n_short - 1) + k
        smoothed = smoothed + short[k : k + 1, :] * ext_r[at : at + length, :]
    rounded = smoothed.astype(bf16)
    retain = jax.nn.sigmoid(jnp.dot(rounded, md[...], preferred_element_type=f32))
    admit = jax.nn.sigmoid(jnp.dot(rounded, mi[...], preferred_element_type=f32))
    log_decay = (-RATE_SCALE * softplus_negated(base[...])) * retain + jump[...]
    decay = jnp.exp(log_decay)
    inflow = jnp.sqrt(expm1_negated(2.0 * log_decay)) * admit * rounded.astype(f32)
    tile = 128
    n_tiles = dbuf.shape[0]
    for n in range(n_tiles):
        used = min(tile, rw - n * tile)
        dbuf[n, :, :used] = decay[:, n * tile : n * tile + used]
        ibuf[n, :, :used] = inflow[:, n * tile : n * tile + used]
    seg = length // SEGS

    def scan_step(j, carry):
        new = []
        for n, (p, s) in enumerate(carry):
            at = (n, pl.ds(j, SEGS, stride=seg), slice(None))
            d, i = dbuf[at], ibuf[at]
            p, s = d * p, d * s + i
            dbuf[at] = p
            ibuf[at] = s
            new.append((p, s))
        return tuple(new)

    start = tuple((jnp.ones((SEGS, tile), f32), jnp.zeros((SEGS, tile), f32)) for _ in range(n_tiles))
    ends = lax.fori_loop(0, seg, scan_step, start)
    p_all = jnp.concatenate([e[0] for e in ends], axis=1)
    s_all = jnp.concatenate([e[1] for e in ends], axis=1)
    half = cy.shape[2] // 2
    p_run, s_run = jnp.ones((1, half), f32), jnp.zeros((1, half), f32)
    before = []
    for g in range(SEGS):
        before.append((p_run, s_run))
        p_g, s_g = p_all[g : g + 1, :], s_all[g : g + 1, :]
        p_run, s_run = p_run * p_g, p_g * s_run + s_g

    def carry_copy(buf, slot, send, recv, d, to):
        return pltpu.make_async_remote_copy(
            src_ref=buf.at[slot], dst_ref=buf.at[slot], send_sem=send.at[d - 1], recv_sem=recv.at[d - 1],
            device_id={"sp": rem(to[0], NZ) * NY + rem(to[1], NY)}, device_id_type=MESH,
        )

    cy[y, :, :half] = p_run
    cy[y, :, half:] = s_run
    for d in range(1, NY):
        carry_copy(cy, y, cy_s, cy_r, d, (z, y + d)).start()

    for d in range(1, NX * NC):
        stat_arrival(d).wait_recv()
    totals = stats[0]
    for n in range(1, NX * NC):
        totals = totals + stats[n]
    scale = 1.0 / CONV_WIDTH
    row_id = lax.broadcasted_iota(jnp.int32, (8, cw), 0)
    mean = lax.dot_general(
        totals * scale, jnp.where(row_id == 0, 1.0, 0.0), TN_DIMS, precision=exact, preferred_element_type=f32
    )
    square = lax.dot_general(
        totals * scale, jnp.where(row_id == 4, 1.0, 0.0), TN_DIMS, precision=exact, preferred_element_type=f32
    )

    for d in range(1, NY):
        carry_copy(cy, rem(y - d, NY), cy_s, cy_r, d, (z, y + d)).wait_recv()
    p_run, s_run = jnp.ones((1, half), f32), jnp.zeros((1, half), f32)
    p_mine, s_mine = p_run, s_run
    for n in range(NY):
        p_mine = jnp.where(y == n, p_run, p_mine)
        s_mine = jnp.where(y == n, s_run, s_mine)
        p_n, s_n = cy[n, :, :half], cy[n, :, half:]
        p_run, s_run = p_run * p_n, p_n * s_run + s_n
    cz[z, :, :half] = p_run
    cz[z, :, half:] = s_run
    for d in range(1, NZ):
        carry_copy(cz, z, cz_s, cz_r, d, (z + d, y)).start()

    spread = jnp.maximum(square - mean * mean, 0.0)
    scaled = (filt[...] - mean) * lax.rsqrt(spread + 1e-05) * cgain[...]
    co[...] = (scaled * jax.nn.sigmoid(scaled)).astype(bf16)
    for k in range(NZ):
        g_out.along_y_last(k)
    block = 512

    def conv_part(j, carry):
        cols = pl.ds(pl.multiple_of(j * block, block), block)
        pc[:, cols] = lax.dot_general(co[...], oc[cols, :], NT_DIMS, preferred_element_type=f32)
        return carry

    lax.fori_loop(0, width // block, conv_part, 0)

    for d in range(1, NZ):
        carry_copy(cz, rem(z - d, NZ), cz_s, cz_r, d, (z + d, y)).wait_recv()
    entering = jnp.zeros((1, half), f32)
    for n in range(NZ):
        entering = jnp.where(n < z, cz[n, :, :half] * entering + cz[n, :, half:], entering)
    entering = p_mine * entering + s_mine
    for g, (p_g, s_g) in enumerate(before):
        part = slice(g * seg, (g + 1) * seg)
        at_start = p_g * entering + s_g
        for n in range(n_tiles):
            used = min(tile, rw - n * tile)
            lanes = slice(n * tile, n * tile + used)
            state = ibuf[n, part, :used] + dbuf[n, part, :used] * at_start[:, lanes]
            ro[part, lanes] = (gbuf[part, lanes] * state).astype(bf16)

    def chip_rows(xx, cc):
        return pl.ds(pl.multiple_of((rem(xx, NX) * NC + rem(cc, NC)) * n_tok, n_tok), n_tok)

    def rec_part(j, carry):
        cols = pl.ds(pl.multiple_of(j * block, block), block)
        pc[:, cols] += lax.dot_general(ro[...], orr[cols, :rw], NT_DIMS, preferred_element_type=f32)
        for d in range(NX):
            ps[d, :, cols] = pc[chip_rows(x + d, c + 1), cols].astype(bf16)
        return carry

    def pair_copy(d, side):
        lanes = (lo, hi)[side]
        return pltpu.make_async_remote_copy(
            src_ref=ps.at[d, :, lanes], dst_ref=pr.at[d, :, lanes],
            send_sem=pr_s.at[2 * d + side], recv_sem=pr_r.at[2 * d + side],
            device_id={"tp": x * NC + rem(c + 1, NC)}, device_id_type=MESH,
        )

    for side in range(2):
        n_blocks = width // block // 2
        lax.fori_loop(side * n_blocks, (side + 1) * n_blocks, rec_part, 0)
        for d in (2, 1, 3, 0):
            pair_copy(d, side).start()

    def x_copy(src, dst, index, xx):
        return pltpu.make_async_remote_copy(
            src_ref=src, dst_ref=dst, send_sem=x_s.at[index], recv_sem=x_r.at[index],
            device_id={"tp": rem(xx, NX) * NC + c}, device_id_type=MESH,
        )

    halves = (slice(0, width // 2), slice(width // 2, width))

    def chip_sum(d, side):
        h = halves[side]
        return pc[chip_rows(x + d, c), h] + pr[d, :, h].astype(f32)

    copies = [
        x_copy(s2.at[:, lo], two.at[:, lo], 0, x + 1),
        x_copy(s2.at[:, hi], two.at[:, hi], 1, x - 1),
        x_copy(sp_buf.at[:, hi], from_m.at[:, hi], 2, x + 1),
        x_copy(sm_buf.at[:, lo], from_p.at[:, lo], 3, x - 1),
        x_copy(sp_buf.at[:, lo], from_m.at[:, lo], 4, x + 1),
        x_copy(sm_buf.at[:, hi], from_p.at[:, hi], 5, x - 1),
    ]
    for side in range(2):
        pair_copy(2, side).wait_recv()
        s2[:, halves[side]] = chip_sum(2, side).astype(bf16)
        copies[side].start()
    pair_copy(3, 0).wait_recv()
    sm_buf[:, halves[0]] = chip_sum(3, 0).astype(bf16)
    copies[3].start()
    pair_copy(1, 1).wait_recv()
    sp_buf[:, halves[1]] = chip_sum(1, 1).astype(bf16)
    copies[2].start()
    pair_copy(1, 0).wait_recv()
    copies[0].wait_recv()
    sp_buf[:, halves[0]] = (chip_sum(1, 0) + two[:, halves[0]].astype(f32)).astype(bf16)
    copies[4].start()
    pair_copy(3, 1).wait_recv()
    copies[1].wait_recv()
    sm_buf[:, halves[1]] = (chip_sum(3, 1) + two[:, halves[1]].astype(f32)).astype(bf16)
    copies[5].start()
    mine = chip_rows(x, c)
    for side in range(2):
        pair_copy(0, side).wait_recv()
        pc[mine, halves[side]] = chip_sum(0, side)
    for n in range(2, 6):
        copies[n].wait_recv()
    out[...] = (pc[mine, :] + (from_m[...].astype(f32) + from_p[...].astype(f32))).astype(bf16)

    g_in.finish()
    g_out.finish()
    for args in t_sent:
        tok_copy(*args).wait_send()
    for e in edges:
        e.wait_send()
    for d in range(1, NX * NC):
        stat_copy(d).wait_send()
    for d in range(1, NY):
        carry_copy(cy, y, cy_s, cy_r, d, (z, y + d)).wait_send()
    for d in range(1, NZ):
        carry_copy(cz, z, cz_s, cz_r, d, (z + d, y)).wait_send()
    for side in range(2):
        for d in range(NX):
            pair_copy(d, side).wait_send()
    for n in copies:
        n.wait_send()


def shards(
    tokens, norm_gain, conv_val_w, conv_gate_w, rec_gate_w, rec_in_w, conv_taps, conv_bias, conv_gain,
    short_taps, decay_map, input_map, decay_base, decay_jump, out_conv_w, out_rec_w,
):
    cw, rw = conv_val_w.shape[1], rec_in_w.shape[1]
    n_tok, width = tokens.shape
    length = n_tok * NX * NC
    wide = rw + -rw % 128
    f32, bf16 = jnp.float32, jnp.bfloat16
    vmem = pl.BlockSpec(memory_space=pltpu.VMEM)
    V, S = pltpu.VMEM, pltpu.SemaphoreType.DMA
    return pl.pallas_call(
        whole_kernel,
        out_shape=jax.ShapeDtypeStruct((n_tok, width), bf16),
        in_specs=[vmem] * 14,
        out_specs=vmem,
        scratch_shapes=[
            V((length, width), bf16),
            V((width, 2 * cw), bf16),
            V((width, 2 * rw), bf16),
            V((length, 2 * cw), f32),
            V((length, 2 * rw), f32),
            V((width, cw), bf16),
            V((width, wide), bf16),
            V((length + 32, cw), f32),
            V((length + 8, rw), f32),
            V((length, cw), f32),
            V((rw, rw), bf16),
            V((rw, rw), bf16),
            V((NX * NC, 8, length), f32),
            V((wide // 128, length, 128), f32),
            V((wide // 128, length, 128), f32),
            V((length, rw), f32),
            V((length, cw), bf16),
            V((length, rw), bf16),
            V((8, 128), f32),
            V((NY, 1, 2 * wide), f32),
            V((NZ, 1, 2 * wide), f32),
            V((length, width), f32),
            V((NX, n_tok, width), bf16),
            V((NX, n_tok, width), bf16),
            V((n_tok, width), bf16),
            V((n_tok, width), bf16),
            V((n_tok, width), bf16),
            V((n_tok, width), bf16),
            V((n_tok, width), bf16),
            V((n_tok, width), bf16),
            *Gather.semaphores(),
            *Gather.semaphores(),
            S((9,)), S((9,)), S((2,)), S((2,)), S((7,)), S((7,)), S((3,)), S((3,)),
            S((NZ - 1,)), S((NZ - 1,)), S((2 * NX,)), S((2 * NX,)), S((6,)), S((6,)),
        ],
        compiler_params=pltpu.CompilerParams(
            collective_id=0, has_side_effects=True, vmem_limit_bytes=60 * 1024 * 1024
        ),
    )(
        tokens,
        norm_gain[None, :],
        jnp.concatenate([conv_val_w, conv_gate_w], axis=1),
        jnp.concatenate([rec_in_w, rec_gate_w], axis=1),
        out_conv_w.T,
        jnp.pad(out_rec_w.T, ((0, 0), (0, wide - rw))),
        conv_taps,
        conv_bias[None, :],
        conv_gain[None, :],
        short_taps,
        decay_map,
        input_map,
        decay_base[None, :],
        decay_jump,
    )


def solution(mesh):
    in_specs = (
        P(("sp", "tp"), None), P(), P("sp", "tp"), P("sp", "tp"), P("sp", "tp"), P("sp", "tp"),
        P(None, "tp"), P("tp"), P("tp"), P(None, "tp"), P("tp", None, None), P("tp", None, None),
        P("tp"), P("sp", "tp"), P("tp", "sp"), P("tp", "sp"),
    )
    return jax.shard_map(
        shards, mesh=mesh, in_specs=in_specs, out_specs=P(("sp", "tp"), None), check_vma=False
    )
```

time: 198 us -> 122 us (0.62)
  waiting for transfers between devices: 47 us -> 0 us
  Pallas kernels: 84.2 us -> 115 us
  starting transfers between devices: 20.4 us -> 0 us
  between operations: 14.4 us -> 0.01 us
  matrix products: 11.4 us -> 0 us
  local copies, waits for them, and re-layouts: 11.3 us -> 4.43 us
  other arithmetic: 7.58 us -> 2.04 us
    reduce_scatter x1 -> x0, waiting for transfers between devices: 32.6 us -> none  [shards(): lax.psum_scatter((lax.dot_general(conv_out, conv_full, nt_dims, preferred...]
    pallas_call x1, Pallas kernels: 84.2 us -> 115 us  [shards(): pl.pallas_call(whole_kernel, out_shape=jax.ShapeDtypeStruct((n_tok, width...]
    all_to_all x2 -> x0, starting transfers between devices: 15.6 us -> none  [sent_to_all(): lax.all_to_all(jnp.broadcast_to(value[None], (count, *value.shape)), axis...]
    all_to_all x2 -> x0, waiting for transfers between devices: 14.3 us -> none  [sent_to_all(): lax.all_to_all(jnp.broadcast_to(value[None], (count, *value.shape)), axis...]
    dot_general x4 -> x0, matrix products: 11.4 us -> none  [the longest x1 5.84 us: shards(): lax.dot_general(rec_out, rec_full[:, :rec_cols], nt_dims, preferred_eleme...]
    slice x81 -> x0, local copies, waits for them, and re-layouts: 6.39 us -> none  [the longest x56 2.23 us: shards(): lax.associative_scan(chain_step, (decay, inflow), axis=0)]
    ppermute x2 -> x0, starting transfers between devices: 4.58 us -> none  [passed_along(): return lax.ppermute(value, axis, pairs)]
    unnamed x13 -> x8, local copies, waits for them, and re-layouts: 1.26 us -> 3.82 us
  transfers between devices with their start and end apart: 5 -> 0, of which waited for: 3 -> 0; matrix products, arithmetic and copies ran while one was open for 8% -> 0% of each run, Pallas kernels for 0% -> 0%
where the time goes in v2:
time: 122 us
  Pallas kernels  115 us (94%)
  local copies, waits for them, and re-layouts  4.43 us (4%)
  other arithmetic  2.04 us (2%)
    pallas_call x1, Pallas kernels, shards(): pl.pallas_call(whole_kernel, out_shape=jax.ShapeDtypeStruct((n_tok, width...  115 us
    unnamed x8, local copies, waits for them, and re-layouts  3.82 us

profile of v2, /device:TPU:1, one launch (start us, length us, event | category | flops | bytes accessed | tf_op | source)
XLA Modules:
  0.0 121.6 jit_solution(7873698863543542868)
XLA Ops:
  0.0 0.0 copy-start.2
  0.0 1.3 %pad_maximum_fusion.1.wc_own = bf16[64,256]{1,0:T(8,128)(2,1)} fusion(bf16[64,128]{1,0:T(8,128)(2,1)} %param.19, bf16[64,128]{1,0:T(8,128)(2,1)} %param.18), kind=kLoop, calls=%fused_computation.1 | loop fusion | flops 65536 | bytes 65536 | tf_op jit(solution)/shard_map/concatenate | solution.py:615
  1.3 0.0 copy-done.2
  1.4 0.0 copy-start
  1.4 0.0 copy-start.1
  1.4 0.6 pad.4.or_own
  2.0 0.1 copy-done
  2.1 0.0 copy-done.1
  2.1 0.7 pad_maximum_fusion.wr_own
  2.8 1.9 %copy.17.jump = f32[384,192]{1,0:T(8,128)} copy(f32[384,192]{0,1:T(8,128)} %param.29) | data formatting | bytes 589824 | tf_op args[13]
  4.7 115.2 %shard_map.154 = bf16[48,4096]{1,0:T(8,128)(2,1)} custom-call(bf16[48,4096]{1,0:T(8,128)(2,1)} %tokens.1, f32[1,4096]{1,0:T(1,128)} %bitcast.7, bf16[64,256]{1,0:T(8,128)(2,1)} %pad_maximum_fusion.1.wc_own, bf16[64,384]{1,0:T(8,128)(2,1)} %pad_maximum_fusion.wr_own, bf16[64,128]{1,0:T(8,128)(2,1)} %bitcast.8, bf16[64,256]{1,0:T(8,128)(2,1)} %pad.4.or_own, ...), custom_call_target="tpu_custom_call" | custom-call | tf_op jit(solution)/shard_map/pallas_call | solution.py:568
  119.9 1.8 %copy.19 = bf16[48,4096]{1,0:T(8,128)(2,1)} copy(bf16[48,4096]{1,0:T(8,128)(2,1)} %shard_map.154) | data formatting | bytes 786432
Async XLA Ops:
  0.0 1.3 %copy-start.2 = (bf16[192,64]{0,1:T(8,128)(2,1)S(1)}, bf16[192,64]{0,1:T(8,128)(2,1)}, u32[]{:S(2)}) copy-start(bf16[192,64]{0,1:T(8,128)(2,1)} %param.31) | copy-start | bytes 73732
  1.4 0.8 copy-start
  1.4 0.8 copy-start.1

commit v3 on v2

v3 whole, which is shorter than its diff:
```python
import jax
import jax.numpy as jnp
from jax import lax
from jax.experimental import pallas as pl
from jax.experimental.pallas import tpu as pltpu
from jax.sharding import PartitionSpec as P

MESH = pl.DeviceIdType.MESH
CONV_WIDTH = 1024
RATE_SCALE = 8.0
NZ, NY, NX, NC = 16, 4, 4, 2
HALF = NZ // 2


def rem(a, n):
    return lax.rem(a + 4 * n, n)


class Gather:
    def __init__(self, a, b, rows, sems, pos):
        self.a, self.b = a, b
        self.rows = {id(a): rows[0], id(b): rows[1]}
        self.s, self.r = sems[: len(sems) // 2], sems[len(sems) // 2 :]
        self.z, self.y = pos
        self.sent = []

    def at(self, ref, z, y):
        rows = self.rows[id(ref)]
        return ref.at[pl.ds(pl.multiple_of((rem(z, NZ) * NY + rem(y, NY)) * rows, rows), rows)]

    def copy(self, ref, chunk, kind, index, to):
        block = self.at(ref, *chunk)
        return pltpu.make_async_remote_copy(
            src_ref=block,
            dst_ref=block,
            send_sem=self.s[kind].at[index],
            recv_sem=self.r[kind].at[index],
            device_id={"sp": rem(to[0], NZ) * NY + rem(to[1], NY)},
            device_id_type=MESH,
        )

    def send(self, *args):
        self.copy(*args).start()
        self.sent.append(args)

    def arrived(self, ref, chunk, kind, index):
        self.copy(ref, chunk, kind, index, (self.z + 1, self.y)).wait_recv()

    def start_y(self):
        z, y, a = self.z, self.y, self.a
        for d in (1, 3, 2):
            self.send(a, (z, y), 0, d - 1, (z, y + d))

    def start_z(self):
        z, y = self.z, self.y
        for ref, up in ((self.b, 3), (self.a, 1)):
            self.send(ref, (z, y), up, 0, (z + 1, y))
            self.send(ref, (z, y), up + 1, 0, (z - 1, y))

    def from_y(self):
        z, y, a = self.z, self.y, self.a
        for d in (1, 3, 2):
            self.arrived(a, (z, y - d), 0, d - 1)
            self.send(a, (z, y - d), 1, d, (z + 1, y))
            self.send(a, (z, y - d), 2, d, (z - 1, y))

    def spread(self, k):
        z, y = self.z, self.y
        self.send(self.b, (z - k, y), 5, 3 * k, (z, y + 1))
        self.send(self.b, (z - k, y), 5, 3 * k + 1, (z, y - 1))
        if k == HALF:
            self.send(self.b, (z - k, y), 5, 3 * k + 2, (z, y + 2))

    def along_z(self, s, between=lambda: None):
        z, y, a, b = self.z, self.y, self.a, self.b
        last, next_last = s == HALF, s + 1 == HALF
        self.arrived(b, (z - s, y), 3, s - 1)
        if not last:
            self.send(b, (z - s, y), 3, s, (z + 1, y))
            self.arrived(b, (z + s, y), 4, s - 1)
            if not next_last:
                self.send(b, (z + s, y), 4, s, (z - 1, y))
            self.spread(s)
            self.spread(NZ - s)
        else:
            self.spread(s)
        for d in (0, 1, 3, 2):
            if not last or d == 0:
                self.arrived(a, (z - s, y - d), 1, 4 * (s - 1) + d)
            if not last and not (next_last and d > 0):
                self.send(a, (z - s, y - d), 1, 4 * s + d, (z + 1, y))
            if not last or d > 0:
                self.arrived(a, (z + s, y - d), 2, 4 * (s - 1) + d)
            if not last and not (next_last and d == 0):
                self.send(a, (z + s, y - d), 2, 4 * s + d, (z - 1, y))
            between()

    def along_y(self, k):
        z, y = self.z, self.y
        turn = 1 - 2 * (k % 2)
        self.arrived(self.b, (z - k, y - 1), 5, 3 * k)
        self.arrived(self.b, (z - k, y + 1), 5, 3 * k + 1)
        if k != HALF:
            self.send(self.b, (z - k, y - turn), 5, 3 * k + 2, (z, y + turn))

    def along_y_last(self, k):
        self.arrived(self.b, (self.z - k, self.y + 2), 5, 3 * k + 2)

    def finish(self):
        for args in self.sent:
            self.copy(*args).wait_send()

    @staticmethod
    def semaphores():
        counts = [3, 4 * HALF, 4 * HALF, HALF, HALF, 3 * NZ]
        return [pltpu.SemaphoreType.DMA((n,)) for n in counts + counts]


N_SEMS = 12


def groups_of(step):
    if step == 0:
        return [0]
    if step < HALF:
        return [step, NZ - step]
    return [step] if step == HALF else []


def expm1_negated(v):
    series = jnp.ones_like(v)
    for n in range(9, 1, -1):
        series = 1.0 + series * v * (1.0 / n)
    return jnp.where(v > -0.5, -v * series, 1.0 - jnp.exp(v))


def softplus_negated(b):
    e = jnp.exp(-jnp.abs(b))
    w = e / (2.0 + e)
    q = w * w
    series = jnp.full_like(w, 1.0 / 15.0)
    for n in (13, 11, 9, 7, 5, 3, 1):
        series = 1.0 / n + series * q
    return jnp.maximum(-b, 0.0) + 2.0 * w * series


NT_DIMS = (((1,), (1,)), ((), ()))
TN_DIMS = (((0,), (0,)), ((), ()))
SEGS = 8


def whole_kernel(
    tokens, gain, wv_own, wg_own, ri_own, rg_own, oc_own, or_own, taps, bias, cgain, staps, dmap, imap, base, jump_t, out, *scratch
):
    (nt, wa, wb, acc_a, acc_b, oc, packed, orr, ext_c, ext_r, filt, md, mi, stats, dbuf, ibuf, gbuf, co, ro,
     jump, cy, cz, pc, ps, pr, s2, sp_buf, sm_buf, two, from_m, from_p) = scratch[:31]
    scratch = scratch[31:]
    sems_in, sems_out = scratch[:N_SEMS], scratch[N_SEMS : 2 * N_SEMS]
    (tok_s, tok_r, edge_s, edge_r, stat_s, stat_r, cy_s, cy_r, cz_s, cz_r, pr_s, pr_r, x_s, x_r) = scratch[2 * N_SEMS :]
    sp, tp = lax.axis_index("sp"), lax.axis_index("tp")
    z, y, x, c = sp // NY, sp % NY, tp // NC, tp % NC
    rows = wv_own.shape[0]
    n_tok, width = tokens.shape
    length = acc_a.shape[0]
    cw, rw = wv_own.shape[1], ri_own.shape[1]
    f32, bf16 = jnp.float32, jnp.bfloat16

    barrier = pltpu.get_barrier_semaphore()
    for dz, dy in ((1, 0), (-1, 0), (0, 1), (0, 2), (0, 3)):
        pl.semaphore_signal(
            barrier, inc=1, device_id={"sp": rem(z + dz, NZ) * NY + rem(y + dy, NY)}, device_id_type=MESH
        )
    for d in (1, -1):
        pl.semaphore_signal(barrier, inc=1, device_id={"sp": rem(sp + d, NZ * NY)}, device_id_type=MESH)
    for d in range(1, NX * NC):
        pl.semaphore_signal(barrier, inc=1, device_id={"tp": rem(tp + d, NX * NC)}, device_id_type=MESH)

    own = pl.ds(pl.multiple_of(sp * rows, rows), rows)
    extra = wa.shape[1] - rw
    wa[own, :] = jnp.concatenate([ri_own[...], rg_own[:, :extra]], axis=1)
    wb[own, :cw] = wv_own[...]
    wb[own, cw : 2 * cw] = wg_own[...]
    wb[own, 2 * cw :] = rg_own[:, extra:]
    oc[own] = oc_own[...]
    p_rows, h_rows = rows + rows // 2, rows // 2
    p_at = pl.multiple_of(sp * p_rows, h_rows)
    packed[pl.ds(p_at, rows)] = or_own[:, :128]
    packed[pl.ds(p_at + rows, h_rows)] = jnp.concatenate([or_own[:h_rows, 128:], or_own[h_rows:, 128:]], axis=1)

    def unpack(k):
        for n in range(NY):
            chunk = rem(z - k, NZ) * NY + n
            src = pl.multiple_of(chunk * p_rows, h_rows)
            dst = pl.multiple_of(chunk * rows, rows)
            orr[pl.ds(dst, rows), :128] = packed[pl.ds(src, rows)]
            pair = packed[pl.ds(src + rows, h_rows)]
            orr[pl.ds(dst, h_rows), 128:rw] = pair[:, : rw - 128]
            orr[pl.ds(dst + h_rows, h_rows), 128:rw] = pair[:, rw - 128 :]

    pl.semaphore_wait(barrier, 7 + NX * NC - 1)

    g_in = Gather(wa, wb, (rows, rows), sems_in, (z, y))
    g_out = Gather(oc, packed, (rows, rows + rows // 2), sems_out, (z, y))
    g_in.start_z()
    g_in.start_y()
    g_in.spread(0)
    g_out.start_z()

    def tok_rows(xx, cc):
        return pl.ds(pl.multiple_of((rem(xx, NX) * NC + rem(cc, NC)) * n_tok, 16), n_tok)

    def tok_at(xx, cc, lanes=None):
        r = tok_rows(xx, cc)
        return nt.at[r] if lanes is None else nt.at[r, lanes]

    def tok_copy(block, index, xx, cc):
        return pltpu.make_async_remote_copy(
            src_ref=block, dst_ref=block, send_sem=tok_s.at[index], recv_sem=tok_r.at[index],
            device_id={"tp": rem(xx, NX) * NC + rem(cc, NC)}, device_id_type=MESH,
        )

    t_sent = []

    def tok_send(*args):
        tok_copy(*args).start()
        t_sent.append(args)

    lo, hi = pl.ds(0, width // 2), pl.ds(width // 2, width // 2)

    widened = tokens[...].astype(f32)
    inverse = lax.rsqrt(jnp.mean(widened * widened, axis=-1, keepdims=True) + 1e-06)
    tok_at(x, c)[...] = (widened * inverse * gain[...]).astype(bf16)
    tok_send(tok_at(x, c), 0, x + 1, c)
    tok_send(tok_at(x, c), 1, x - 1, c)
    tok_send(tok_at(x, c), 4, x, c + 1)
    g_in.from_y()
    g_out.start_y()
    acc_a[...] = jnp.zeros_like(acc_a)
    acc_b[...] = jnp.zeros_like(acc_b)
    cy[...] = jnp.zeros_like(cy)
    cz[...] = jnp.zeros_like(cz)
    head = dmap.shape[1]
    for m, given in ((md, dmap), (mi, imap)):
        m[...] = jnp.zeros_like(m)
        for h in range(dmap.shape[0]):
            m[h * head : (h + 1) * head, h * head : (h + 1) * head] = given[h]
    jump[...] = jnp.transpose(jump_t[...])

    def tokens_forward():
        tok_copy(tok_at(x - 1, c), 0, x + 1, c).wait_recv()
        tok_send(tok_at(x - 1, c, lo), 2, x + 1, c)
        tok_send(tok_at(x - 1, c), 5, x, c + 1)
        tok_copy(tok_at(x + 1, c), 1, x + 1, c).wait_recv()
        tok_send(tok_at(x + 1, c, hi), 3, x - 1, c)
        tok_send(tok_at(x + 1, c), 6, x, c + 1)

    def tokens_relay():
        tok_copy(tok_at(x + 2, c, lo), 2, x + 1, c).wait_recv()
        tok_send(tok_at(x + 2, c, lo), 7, x, c + 1)
        tok_copy(tok_at(x + 2, c, hi), 3, x + 1, c).wait_recv()
        tok_send(tok_at(x + 2, c, hi), 8, x, c + 1)

    def tokens_last():
        tok_copy(tok_at(x, c + 1), 4, x + 1, c).wait_recv()
        tok_copy(tok_at(x - 1, c + 1), 5, x + 1, c).wait_recv()
        tok_copy(tok_at(x + 1, c + 1), 6, x + 1, c).wait_recv()
        tok_copy(tok_at(x + 2, c + 1, lo), 7, x + 1, c).wait_recv()
        tok_copy(tok_at(x + 2, c + 1, hi), 8, x + 1, c).wait_recv()

    def multiply(acc, w, first, last):
        def body(j, carry):
            s = (j + 1) // 2
            zz = rem(z + jnp.where(j % 2 == 1, -s, s), NZ)
            cols = pl.ds(pl.multiple_of(zz * (NY * rows), NY * rows), NY * rows)
            acc[...] += jnp.dot(nt[:, cols], w[cols, :], preferred_element_type=f32)
            return carry

        lax.fori_loop(first, last, body, 0)

    a_part = lambda first, last: (lambda: multiply(acc_a, wa, first, last))
    b_part = lambda first, last: (lambda: multiply(acc_b, wb, first, last))
    work = {
        6: [a_part(0, 2), a_part(2, 4), a_part(4, 6), a_part(6, 8)],
        7: [a_part(8, 10), a_part(10, 12), b_part(0, 2), b_part(2, 4)],
        8: [b_part(4, 6), b_part(6, 8), b_part(8, 10), a_part(12, 15)],
    }

    def out_step(s):
        if s == 0:
            g_out.spread(0)
            g_out.from_y()
        elif s <= HALF:
            g_out.along_z(s)
        if s >= 1:
            for k in groups_of(s - 1):
                g_out.along_y(k)
        if s >= 2:
            for k in groups_of(s - 2):
                g_out.along_y_last(k)
                unpack(k)

    lag = 4

    def at_step(step):
        todo = list(work.get(step, []))
        g_in.along_z(step, lambda: todo and todo.pop(0)())
        if step == HALF:
            a_part(NZ - 1, NZ)()
            start_recurrence()
        for k in groups_of(step - 1):
            g_in.along_y(k)
        if step >= lag:
            out_step(step - lag)
        if step >= 2:
            for k in groups_of(step - 2):
                g_in.along_y_last(k)
        if step == 2:
            tokens_forward()
        if step == 4:
            tokens_relay()
        if step == 5:
            tokens_last()

    c_pad, r_pad = ext_c.shape[0] - length, ext_r.shape[0] - length

    def edge_copy(ref, pad, index):
        return pltpu.make_async_remote_copy(
            src_ref=ref.at[pl.ds(length, pad)], dst_ref=ref.at[pl.ds(0, pad)],
            send_sem=edge_s.at[index], recv_sem=edge_r.at[index],
            device_id={"sp": rem(sp + 1, NZ * NY)}, device_id_type=MESH,
        )

    edges = [edge_copy(ext_r, r_pad, 0), edge_copy(ext_c, c_pad, 1)]

    def take_edge(index, ref, pad):
        edges[index].wait_recv()
        ref[:pad, :] = jnp.where(sp > 0, ref[:pad, :], 0.0)

    def start_recurrence():
        ext_r[r_pad:, :] = acc_a[:, :rw].astype(bf16).astype(f32)
        edges[0].start()

    for step in range(1, HALF + 1):
        at_step(step)

    n_short = staps.shape[0]
    short = staps[...].astype(f32)
    rate = -RATE_SCALE * softplus_negated(base[...])
    tile = 128
    n_tiles = dbuf.shape[0]

    def gates(first, count):
        smoothed = jnp.zeros((count, rw), f32)
        for k in range(n_short):
            at = r_pad - (n_short - 1) + k + first
            smoothed = smoothed + short[k : k + 1, :] * ext_r[at : at + count, :]
        rounded = smoothed.astype(bf16)
        retain = jax.nn.sigmoid(jnp.dot(rounded, md[...], preferred_element_type=f32))
        admit = jax.nn.sigmoid(jnp.dot(rounded, mi[...], preferred_element_type=f32))
        log_decay = rate * retain + jump[first : first + count, :]
        decay = jnp.exp(log_decay)
        inflow = jnp.sqrt(expm1_negated(2.0 * log_decay)) * admit * rounded.astype(f32)
        for n in range(n_tiles):
            used = min(tile, rw - n * tile)
            dbuf[n, first : first + count, :used] = decay[:, n * tile : n * tile + used]
            ibuf[n, first : first + count, :used] = inflow[:, n * tile : n * tile + used]

    early = 16
    gates(early, length - early)
    b_part(10, 13)()
    out_step(HALF + 1 - lag)
    take_edge(0, ext_r, r_pad)
    gates(0, early)
    seg = length // SEGS

    def scan_step(j, carry):
        new = []
        for n, (p, s) in enumerate(carry):
            at = (n, pl.ds(j, SEGS, stride=seg), slice(None))
            d, i = dbuf[at], ibuf[at]
            p, s = d * p, d * s + i
            dbuf[at] = p
            ibuf[at] = s
            new.append((p, s))
        return tuple(new)

    start = tuple((jnp.ones((SEGS, tile), f32), jnp.zeros((SEGS, tile), f32)) for _ in range(n_tiles))
    ends = lax.fori_loop(0, seg, scan_step, start)
    p_all = jnp.concatenate([e[0] for e in ends], axis=1)
    s_all = jnp.concatenate([e[1] for e in ends], axis=1)
    half = cy.shape[2] // 2
    p_run, s_run = jnp.ones((1, half), f32), jnp.zeros((1, half), f32)
    before = []
    for g in range(SEGS):
        before.append((p_run, s_run))
        p_g, s_g = p_all[g : g + 1, :], s_all[g : g + 1, :]
        p_run, s_run = p_run * p_g, p_g * s_run + s_g

    def carry_copy(buf, slot, send, recv, d, to):
        return pltpu.make_async_remote_copy(
            src_ref=buf.at[slot], dst_ref=buf.at[slot], send_sem=send.at[d - 1], recv_sem=recv.at[d - 1],
            device_id={"sp": rem(to[0], NZ) * NY + rem(to[1], NY)}, device_id_type=MESH,
        )

    cy[y, :, :half] = p_run
    cy[y, :, half:] = s_run
    for d in range(1, NY):
        carry_copy(cy, y, cy_s, cy_r, d, (z, y + d)).start()
    for k in groups_of(HALF):
        g_in.along_y(k)
    for k in groups_of(HALF - 1) + groups_of(HALF):
        g_in.along_y_last(k)
    b_part(13, NZ)()
    conv_val = acc_b[:, :cw].astype(bf16).astype(f32)
    conv_gate = acc_b[:, cw : 2 * cw].astype(bf16).astype(f32)
    ext_c[c_pad:, :] = (conv_val * jax.nn.sigmoid(conv_gate)).astype(bf16).astype(f32)
    edges[1].start()
    gate = jnp.concatenate([acc_a[:, rw:], acc_b[:, 2 * cw :]], axis=1).astype(bf16).astype(f32)
    gbuf[...] = 0.5 * gate * (1.0 + jnp.tanh(0.7978845608028654 * (gate + 0.044715 * gate * gate * gate)))
    out_step(HALF + 2 - lag)
    n_taps = taps.shape[0]
    wide = taps[...].astype(f32)
    tap_rows = 32

    def filter_rows(first):
        total = jnp.broadcast_to(bias[...], (tap_rows, cw))
        for k in range(n_taps):
            at = first + c_pad - (n_taps - 1) + k
            total = total + wide[k : k + 1, :] * ext_c[at : at + tap_rows, :]
        filt[first : first + tap_rows, :] = total

    for i in range(1, length // tap_rows):
        filter_rows(i * tap_rows)
    for d in range(1, NY):
        carry_copy(cy, rem(y - d, NY), cy_s, cy_r, d, (z, y + d)).wait_recv()
    p_run, s_run = jnp.ones((1, half), f32), jnp.zeros((1, half), f32)
    p_mine, s_mine = p_run, s_run
    for n in range(NY):
        p_mine = jnp.where(y == n, p_run, p_mine)
        s_mine = jnp.where(y == n, s_run, s_mine)
        p_n, s_n = cy[n, :, :half], cy[n, :, half:]
        p_run, s_run = p_run * p_n, p_n * s_run + s_n
    cz[z, :, :half] = p_run
    cz[z, :, half:] = s_run
    for d in range(1, NZ):
        carry_copy(cz, z, cz_s, cz_r, d, (z + d, y)).start()
    take_edge(1, ext_c, c_pad)
    filter_rows(0)
    filtered = filt[...]
    row_id = lax.broadcasted_iota(jnp.int32, (8, cw), 0)
    first_half = jnp.where(row_id < 4, 1.0, 0.0)
    exact = lax.Precision.HIGHEST
    stats[tp] = lax.dot_general(
        first_half, filtered, NT_DIMS, precision=exact, preferred_element_type=f32
    ) + lax.dot_general(
        1.0 - first_half, filtered * filtered, NT_DIMS, precision=exact, preferred_element_type=f32
    )

    def stat_copy(d):
        return pltpu.make_async_remote_copy(
            src_ref=stats.at[tp], dst_ref=stats.at[tp], send_sem=stat_s.at[d - 1], recv_sem=stat_r.at[d - 1],
            device_id={"tp": rem(tp + d, NX * NC)}, device_id_type=MESH,
        )

    def stat_arrival(d):
        slot = stats.at[rem(tp - d, NX * NC)]
        return pltpu.make_async_remote_copy(
            src_ref=slot, dst_ref=slot, send_sem=stat_s.at[d - 1], recv_sem=stat_r.at[d - 1],
            device_id={"tp": rem(tp + d, NX * NC)}, device_id_type=MESH,
        )

    for d in range(1, NX * NC):
        stat_copy(d).start()

    out_step(HALF + 3 - lag)
    for d in range(1, NX * NC):
        stat_arrival(d).wait_recv()
    totals = stats[0]
    for n in range(1, NX * NC):
        totals = totals + stats[n]
    scale = 1.0 / CONV_WIDTH
    row_id = lax.broadcasted_iota(jnp.int32, (8, cw), 0)
    mean = lax.dot_general(
        totals * scale, jnp.where(row_id == 0, 1.0, 0.0), TN_DIMS, precision=exact, preferred_element_type=f32
    )
    square = lax.dot_general(
        totals * scale, jnp.where(row_id == 4, 1.0, 0.0), TN_DIMS, precision=exact, preferred_element_type=f32
    )
    spread = jnp.maximum(square - mean * mean, 0.0)
    scaled = (filt[...] - mean) * lax.rsqrt(spread + 1e-05) * cgain[...]
    co[...] = (scaled * jax.nn.sigmoid(scaled)).astype(bf16)
    out_step(HALF + 4 - lag)
    block = 512

    def conv_part(j, carry):
        cols = pl.ds(pl.multiple_of(j * block, block), block)
        pc[:, cols] = lax.dot_general(co[...], oc[cols, :], NT_DIMS, preferred_element_type=f32)
        return carry

    lax.fori_loop(0, width // block, conv_part, 0)
    out_step(HALF + 5 - lag)
    for s in range(max(HALF + 6 - lag, 0), HALF + 3):
        out_step(s)
    for d in range(1, NZ):
        carry_copy(cz, rem(z - d, NZ), cz_s, cz_r, d, (z + d, y)).wait_recv()
    entering = jnp.zeros((1, half), f32)
    for n in range(NZ):
        entering = jnp.where(n < z, cz[n, :, :half] * entering + cz[n, :, half:], entering)
    entering = p_mine * entering + s_mine
    for g, (p_g, s_g) in enumerate(before):
        part = slice(g * seg, (g + 1) * seg)
        at_start = p_g * entering + s_g
        for n in range(n_tiles):
            used = min(tile, rw - n * tile)
            lanes = slice(n * tile, n * tile + used)
            state = ibuf[n, part, :used] + dbuf[n, part, :used] * at_start[:, lanes]
            ro[part, lanes] = (gbuf[part, lanes] * state).astype(bf16)

    def chip_rows(xx, cc):
        return pl.ds(pl.multiple_of((rem(xx, NX) * NC + rem(cc, NC)) * n_tok, n_tok), n_tok)

    def rec_part(j, carry):
        cols = pl.ds(pl.multiple_of(j * block, block), block)
        pc[:, cols] += lax.dot_general(ro[...], orr[cols, :rw], NT_DIMS, preferred_element_type=f32)
        for d in range(NX):
            ps[d, :, cols] = pc[chip_rows(x + d, c + 1), cols].astype(bf16)
        return carry

    quarter = width // 4

    def lanes_of(q):
        return slice(q * quarter, (q + 1) * quarter)

    def pair_copy(d, q):
        lanes = lanes_of(q)
        return pltpu.make_async_remote_copy(
            src_ref=ps.at[d, :, lanes], dst_ref=pr.at[d, :, lanes],
            send_sem=pr_s.at[4 * d + q], recv_sem=pr_r.at[4 * d + q],
            device_id={"tp": x * NC + rem(c + 1, NC)}, device_id_type=MESH,
        )

    def project(q):
        n_blocks = quarter // block
        lax.fori_loop(q * n_blocks, (q + 1) * n_blocks, rec_part, 0)
        for d in (2, 1, 3, 0):
            pair_copy(d, q).start()

    def x_copy(src, dst, index, q, xx):
        return pltpu.make_async_remote_copy(
            src_ref=src.at[:, lanes_of(q)], dst_ref=dst.at[:, lanes_of(q)],
            send_sem=x_s.at[index], recv_sem=x_r.at[index],
            device_id={"tp": rem(xx, NX) * NC + c}, device_id_type=MESH,
        )

    def chip_sum(d, q):
        pair_copy(d, q).wait_recv()
        return pc[chip_rows(x + d, c), lanes_of(q)] + pr[d, :, lanes_of(q)].astype(f32)

    far = [x_copy(s2, two, q, q, x + 1 if q < 2 else x - 1) for q in range(4)]
    up = [x_copy(sp_buf, from_m, 4 + q, q, x + 1) for q in range(4)]
    down = [x_copy(sm_buf, from_p, 8 + q, q, x - 1) for q in range(4)]

    def send_far(q):
        s2[:, lanes_of(q)] = chip_sum(2, q).astype(bf16)
        far[q].start()

    def send_near(d, q):
        buf, copies = (sp_buf, up) if d == 1 else (sm_buf, down)
        total = chip_sum(d, q)
        if (q < 2) == (d == 1):
            far[q].wait_recv()
            total = total + two[:, lanes_of(q)].astype(f32)
        buf[:, lanes_of(q)] = total.astype(bf16)
        copies[q].start()

    project(0)
    project(2)
    send_far(0)
    send_far(2)
    project(1)
    project(3)
    send_near(3, 0)
    send_near(1, 2)
    send_far(1)
    send_far(3)
    send_near(3, 1)
    send_near(1, 3)
    send_near(1, 0)
    send_near(3, 2)
    send_near(1, 1)
    send_near(3, 3)
    mine = chip_rows(x, c)
    for q in range(4):
        pc[mine, lanes_of(q)] = chip_sum(0, q)
    for q in (0, 2, 1, 3):
        at = lanes_of(q)
        up[q].wait_recv()
        down[q].wait_recv()
        out[:, at] = (pc[mine, at] + (from_m[:, at].astype(f32) + from_p[:, at].astype(f32))).astype(bf16)

    g_in.finish()
    g_out.finish()
    for args in t_sent:
        tok_copy(*args).wait_send()
    for e in edges:
        e.wait_send()
    for d in range(1, NX * NC):
        stat_copy(d).wait_send()
    for d in range(1, NY):
        carry_copy(cy, y, cy_s, cy_r, d, (z, y + d)).wait_send()
    for d in range(1, NZ):
        carry_copy(cz, z, cz_s, cz_r, d, (z + d, y)).wait_send()
    for q in range(4):
        for d in range(NX):
            pair_copy(d, q).wait_send()
    for n in far + up + down:
        n.wait_send()


def shards(
    tokens, norm_gain, conv_val_w, conv_gate_w, rec_gate_w, rec_in_w, conv_taps, conv_bias, conv_gain,
    short_taps, decay_map, input_map, decay_base, decay_jump, out_conv_w, out_rec_w,
):
    cw, rw = conv_val_w.shape[1], rec_in_w.shape[1]
    n_tok, width = tokens.shape
    length = n_tok * NX * NC
    wide = rw + -rw % 128
    f32, bf16 = jnp.float32, jnp.bfloat16
    vmem = pl.BlockSpec(memory_space=pltpu.VMEM)
    V, S = pltpu.VMEM, pltpu.SemaphoreType.DMA
    return pl.pallas_call(
        whole_kernel,
        out_shape=jax.ShapeDtypeStruct((n_tok, width), bf16),
        in_specs=[vmem] * 16,
        out_specs=vmem,
        scratch_shapes=[
            V((length, width), bf16),
            V((width, 2 * cw), bf16),
            V((width, 2 * rw), bf16),
            V((length, 2 * cw), f32),
            V((length, 2 * rw), f32),
            V((width, cw), bf16),
            V((width * 3 // 2, 128), bf16),
            V((width, wide), bf16),
            V((length + 32, cw), f32),
            V((length + 8, rw), f32),
            V((length, cw), f32),
            V((rw, rw), bf16),
            V((rw, rw), bf16),
            V((NX * NC, 8, length), f32),
            V((wide // 128, length, 128), f32),
            V((wide // 128, length, 128), f32),
            V((length, rw), f32),
            V((length, cw), bf16),
            V((length, rw), bf16),
            V((length, rw), f32),
            V((NY, 1, 2 * wide), f32),
            V((NZ, 1, 2 * wide), f32),
            V((length, width), f32),
            V((NX, n_tok, width), bf16),
            V((NX, n_tok, width), bf16),
            V((n_tok, width), bf16),
            V((n_tok, width), bf16),
            V((n_tok, width), bf16),
            V((n_tok, width), bf16),
            V((n_tok, width), bf16),
            V((n_tok, width), bf16),
            *Gather.semaphores(),
            *Gather.semaphores(),
            S((9,)), S((9,)), S((2,)), S((2,)), S((7,)), S((7,)), S((3,)), S((3,)),
            S((NZ - 1,)), S((NZ - 1,)), S((4 * NX,)), S((4 * NX,)), S((12,)), S((12,)),
        ],
        compiler_params=pltpu.CompilerParams(
            collective_id=0, has_side_effects=True, vmem_limit_bytes=60 * 1024 * 1024
        ),
    )(
        tokens,
        norm_gain[None, :],
        conv_val_w,
        conv_gate_w,
        rec_in_w,
        rec_gate_w,
        out_conv_w.T,
        out_rec_w.T,
        conv_taps,
        conv_bias[None, :],
        conv_gain[None, :],
        short_taps,
        decay_map,
        input_map,
        decay_base[None, :],
        decay_jump.T,
    )


def solution(mesh):
    in_specs = (
        P(("sp", "tp"), None), P(), P("sp", "tp"), P("sp", "tp"), P("sp", "tp"), P("sp", "tp"),
        P(None, "tp"), P("tp"), P("tp"), P(None, "tp"), P("tp", None, None), P("tp", None, None),
        P("tp"), P("sp", "tp"), P("tp", "sp"), P("tp", "sp"),
    )
    return jax.shard_map(
        shards, mesh=mesh, in_specs=in_specs, out_specs=P(("sp", "tp"), None), check_vma=False
    )
```

time: 122 us -> 101 us (0.83)
  Pallas kernels: 115 us -> 99.4 us
  local copies, waits for them, and re-layouts: 4.43 us -> 1.77 us
  other arithmetic: 2.04 us -> 0 us
    pallas_call x1, Pallas kernels: 115 us -> 99.4 us  [shards(): pl.pallas_call(whole_kernel, out_shape=jax.ShapeDtypeStruct((n_tok, width...]
    unnamed x8 -> x1, local copies, waits for them, and re-layouts: 3.82 us -> 1.77 us
    concatenate x2 -> x0, other arithmetic: 2.04 us -> none  [the longest x1 1.34 us: shards(): jnp.concatenate([conv_val_w, conv_gate_w], axis=1)]
where the time goes in v3:
time: 101 us
  Pallas kernels  99.4 us (98%)
  local copies, waits for them, and re-layouts  1.77 us (2%)
    pallas_call x1, Pallas kernels, shards(): pl.pallas_call(whole_kernel, out_shape=jax.ShapeDtypeStruct((n_tok, width...  99.4 us

profile of v3, /device:TPU:1, one launch (start us, length us, event | category | flops | bytes accessed | tf_op | source)
XLA Modules:
  0.0 101.1 jit_solution(9987951991952806573)
XLA Ops:
  0.0 99.4 %shard_map.154 = bf16[48,4096]{1,0:T(8,128)(2,1)} custom-call(bf16[48,4096]{1,0:T(8,128)(2,1)} %tokens.1, f32[1,4096]{1,0:T(1,128)} %bitcast.9, bf16[64,128]{1,0:T(8,128)(2,1)} %wv_own.1, bf16[64,128]{1,0:T(8,128)(2,1)} %wg_own.1, bf16[64,192]{1,0:T(8,128)(2,1)} %ri_own.1, bf16[64,192]{1,0:T(8,128)(2,1)} %rg_own.1, bf16[64,128]{1,0:T(8,128)(2,1)} %bitcast.10, ...), custom_call_target="tpu_custom_call" | custom-call | tf_op jit(solution)/shard_map/pallas_call | solution.py:631
  99.4 1.8 %copy.18 = bf16[48,4096]{1,0:T(8,128)(2,1)} copy(bf16[48,4096]{1,0:T(8,128)(2,1)} %shard_map.154) | data formatting | bytes 786432

commit v4 on v3

--- a/solution.py
+++ b/solution.py
@@ -20,9 +20,9 @@
     def __init__(self, a, b, rows, sems, pos):
         self.a, self.b = a, b
         self.rows = {id(a): rows[0], id(b): rows[1]}
-        self.s, self.r = sems[: len(sems) // 2], sems[len(sems) // 2 :]
+        self.s, self.r = {id(a): sems[0], id(b): sems[1]}, sems[2:]
         self.z, self.y = pos
-        self.sent = []
+        self.sent = {id(a): 0, id(b): 0}
 
     def at(self, ref, z, y):
         rows = self.rows[id(ref)]
@@ -33,7 +33,7 @@
         return pltpu.make_async_remote_copy(
             src_ref=block,
             dst_ref=block,
-            send_sem=self.s[kind].at[index],
+            send_sem=self.s[id(ref)].at[0],
             recv_sem=self.r[kind].at[index],
             device_id={"sp": rem(to[0], NZ) * NY + rem(to[1], NY)},
             device_id_type=MESH,
@@ -41,7 +41,7 @@
 
     def send(self, *args):
         self.copy(*args).start()
-        self.sent.append(args)
+        self.sent[id(args[0])] += 1
 
     def arrived(self, ref, chunk, kind, index):
         self.copy(ref, chunk, kind, index, (self.z + 1, self.y)).wait_recv()
@@ -73,26 +73,26 @@
 
     def along_z(self, s, between=lambda: None):
         z, y, a, b = self.z, self.y, self.a, self.b
-        last, next_last = s == HALF, s + 1 == HALF
+        last = s == HALF
         self.arrived(b, (z - s, y), 3, s - 1)
         if not last:
             self.send(b, (z - s, y), 3, s, (z + 1, y))
+        if not last:
             self.arrived(b, (z + s, y), 4, s - 1)
-            if not next_last:
+            if s + 1 < HALF:
                 self.send(b, (z + s, y), 4, s, (z - 1, y))
-            self.spread(s)
+        self.spread(s)
+        if not last:
             self.spread(NZ - s)
-        else:
-            self.spread(s)
         for d in (0, 1, 3, 2):
             if not last or d == 0:
                 self.arrived(a, (z - s, y - d), 1, 4 * (s - 1) + d)
-            if not last and not (next_last and d > 0):
-                self.send(a, (z - s, y - d), 1, 4 * s + d, (z + 1, y))
+                if s + 1 < HALF or s + 1 == HALF and d == 0:
+                    self.send(a, (z - s, y - d), 1, 4 * s + d, (z + 1, y))
             if not last or d > 0:
                 self.arrived(a, (z + s, y - d), 2, 4 * (s - 1) + d)
-            if not last and not (next_last and d == 0):
-                self.send(a, (z + s, y - d), 2, 4 * s + d, (z - 1, y))
+                if s + 1 < HALF or s + 1 == HALF and d > 0:
+                    self.send(a, (z + s, y - d), 2, 4 * s + d, (z - 1, y))
             between()
 
     def along_y(self, k):
@@ -107,16 +107,20 @@
         self.arrived(self.b, (self.z - k, self.y + 2), 5, 3 * k + 2)
 
     def finish(self):
-        for args in self.sent:
-            self.copy(*args).wait_send()
+        for ref in (self.a, self.b):
+            everything = ref.at[pl.ds(0, self.sent[id(ref)] * self.rows[id(ref)])]
+            pltpu.make_async_remote_copy(
+                src_ref=everything, dst_ref=everything, send_sem=self.s[id(ref)].at[0], recv_sem=self.r[0].at[0],
+                device_id={"sp": rem(self.z + 1, NZ) * NY + self.y}, device_id_type=MESH,
+            ).wait_send()
 
     @staticmethod
     def semaphores():
-        counts = [3, 4 * HALF, 4 * HALF, HALF, HALF, 3 * NZ]
-        return [pltpu.SemaphoreType.DMA((n,)) for n in counts + counts]
-
-
-N_SEMS = 12
+        counts = [1, 1, 3, 4 * HALF, 4 * HALF, HALF, HALF, 3 * NZ]
+        return [pltpu.SemaphoreType.DMA((n,)) for n in counts]
+
+
+N_SEMS = 8
 
 
 def groups_of(step):
@@ -215,15 +219,12 @@
 
     def tok_copy(block, index, xx, cc):
         return pltpu.make_async_remote_copy(
-            src_ref=block, dst_ref=block, send_sem=tok_s.at[index], recv_sem=tok_r.at[index],
+            src_ref=block, dst_ref=block, send_sem=tok_s.at[0], recv_sem=tok_r.at[index],
             device_id={"tp": rem(xx, NX) * NC + rem(cc, NC)}, device_id_type=MESH,
         )
-
-    t_sent = []
 
     def tok_send(*args):
         tok_copy(*args).start()
-        t_sent.append(args)
 
     lo, hi = pl.ds(0, width // 2), pl.ds(width // 2, width // 2)
 
@@ -299,7 +300,7 @@
                 g_out.along_y_last(k)
                 unpack(k)
 
-    lag = 4
+    lag = 3
 
     def at_step(step):
         todo = list(work.get(step, []))
@@ -368,7 +369,6 @@
     early = 16
     gates(early, length - early)
     b_part(10, 13)()
-    out_step(HALF + 1 - lag)
     take_edge(0, ext_r, r_pad)
     gates(0, early)
     seg = length // SEGS
@@ -396,16 +396,17 @@
         p_g, s_g = p_all[g : g + 1, :], s_all[g : g + 1, :]
         p_run, s_run = p_run * p_g, p_g * s_run + s_g
 
-    def carry_copy(buf, slot, send, recv, d, to):
+    def carry_copy(buf, slot, send, recv, to):
         return pltpu.make_async_remote_copy(
-            src_ref=buf.at[slot], dst_ref=buf.at[slot], send_sem=send.at[d - 1], recv_sem=recv.at[d - 1],
+            src_ref=buf.at[slot], dst_ref=buf.at[slot], send_sem=send.at[0], recv_sem=recv.at[0],
             device_id={"sp": rem(to[0], NZ) * NY + rem(to[1], NY)}, device_id_type=MESH,
         )
 
     cy[y, :, :half] = p_run
     cy[y, :, half:] = s_run
     for d in range(1, NY):
-        carry_copy(cy, y, cy_s, cy_r, d, (z, y + d)).start()
+        carry_copy(cy, pl.ds(y, 1), cy_s, cy_r, (z, y + d)).start()
+    out_step(HALF + 1 - lag)
     for k in groups_of(HALF):
         g_in.along_y(k)
     for k in groups_of(HALF - 1) + groups_of(HALF):
@@ -417,22 +418,7 @@
     edges[1].start()
     gate = jnp.concatenate([acc_a[:, rw:], acc_b[:, 2 * cw :]], axis=1).astype(bf16).astype(f32)
     gbuf[...] = 0.5 * gate * (1.0 + jnp.tanh(0.7978845608028654 * (gate + 0.044715 * gate * gate * gate)))
-    out_step(HALF + 2 - lag)
-    n_taps = taps.shape[0]
-    wide = taps[...].astype(f32)
-    tap_rows = 32
-
-    def filter_rows(first):
-        total = jnp.broadcast_to(bias[...], (tap_rows, cw))
-        for k in range(n_taps):
-            at = first + c_pad - (n_taps - 1) + k
-            total = total + wide[k : k + 1, :] * ext_c[at : at + tap_rows, :]
-        filt[first : first + tap_rows, :] = total
-
-    for i in range(1, length // tap_rows):
-        filter_rows(i * tap_rows)
-    for d in range(1, NY):
-        carry_copy(cy, rem(y - d, NY), cy_s, cy_r, d, (z, y + d)).wait_recv()
+    carry_copy(cy, pl.ds(0, NY - 1), cy_s, cy_r, (z, y + 1)).wait_recv()
     p_run, s_run = jnp.ones((1, half), f32), jnp.zeros((1, half), f32)
     p_mine, s_mine = p_run, s_run
     for n in range(NY):
@@ -443,7 +429,21 @@
     cz[z, :, :half] = p_run
     cz[z, :, half:] = s_run
     for d in range(1, NZ):
-        carry_copy(cz, z, cz_s, cz_r, d, (z + d, y)).start()
+        carry_copy(cz, pl.ds(z, 1), cz_s, cz_r, (z + d, y)).start()
+    out_step(HALF + 2 - lag)
+    n_taps = taps.shape[0]
+    wide = taps[...].astype(f32)
+    tap_rows = 32
+
+    def filter_rows(first):
+        total = jnp.broadcast_to(bias[...], (tap_rows, cw))
+        for k in range(n_taps):
+            at = first + c_pad - (n_taps - 1) + k
+            total = total + wide[k : k + 1, :] * ext_c[at : at + tap_rows, :]
+        filt[first : first + tap_rows, :] = total
+
+    for i in range(1, length // tap_rows):
+        filter_rows(i * tap_rows)
     take_edge(1, ext_c, c_pad)
     filter_rows(0)
     filtered = filt[...]
@@ -458,23 +458,21 @@
 
     def stat_copy(d):
         return pltpu.make_async_remote_copy(
-            src_ref=stats.at[tp], dst_ref=stats.at[tp], send_sem=stat_s.at[d - 1], recv_sem=stat_r.at[d - 1],
+            src_ref=stats.at[tp], dst_ref=stats.at[tp], send_sem=stat_s.at[0], recv_sem=stat_r.at[0],
             device_id={"tp": rem(tp + d, NX * NC)}, device_id_type=MESH,
         )
 
-    def stat_arrival(d):
-        slot = stats.at[rem(tp - d, NX * NC)]
-        return pltpu.make_async_remote_copy(
-            src_ref=slot, dst_ref=slot, send_sem=stat_s.at[d - 1], recv_sem=stat_r.at[d - 1],
-            device_id={"tp": rem(tp + d, NX * NC)}, device_id_type=MESH,
-        )
+    stats_of_others = pltpu.make_async_remote_copy(
+        src_ref=stats.at[pl.ds(0, NX * NC - 1)], dst_ref=stats.at[pl.ds(0, NX * NC - 1)],
+        send_sem=stat_s.at[0], recv_sem=stat_r.at[0],
+        device_id={"tp": rem(tp + 1, NX * NC)}, device_id_type=MESH,
+    )
 
     for d in range(1, NX * NC):
         stat_copy(d).start()
 
     out_step(HALF + 3 - lag)
-    for d in range(1, NX * NC):
-        stat_arrival(d).wait_recv()
+    stats_of_others.wait_recv()
     totals = stats[0]
     for n in range(1, NX * NC):
         totals = totals + stats[n]
@@ -490,19 +488,10 @@
     scaled = (filt[...] - mean) * lax.rsqrt(spread + 1e-05) * cgain[...]
     co[...] = (scaled * jax.nn.sigmoid(scaled)).astype(bf16)
     out_step(HALF + 4 - lag)
-    block = 512
-
-    def conv_part(j, carry):
-        cols = pl.ds(pl.multiple_of(j * block, block), block)
-        pc[:, cols] = lax.dot_general(co[...], oc[cols, :], NT_DIMS, preferred_element_type=f32)
-        return carry
-
-    lax.fori_loop(0, width // block, conv_part, 0)
     out_step(HALF + 5 - lag)
     for s in range(max(HALF + 6 - lag, 0), HALF + 3):
         out_step(s)
-    for d in range(1, NZ):
-        carry_copy(cz, rem(z - d, NZ), cz_s, cz_r, d, (z + d, y)).wait_recv()
+    carry_copy(cz, pl.ds(0, NZ - 1), cz_s, cz_r, (z + 1, y)).wait_recv()
     entering = jnp.zeros((1, half), f32)
     for n in range(NZ):
         entering = jnp.where(n < z, cz[n, :, :half] * entering + cz[n, :, half:], entering)
@@ -519,9 +508,13 @@
     def chip_rows(xx, cc):
         return pl.ds(pl.multiple_of((rem(xx, NX) * NC + rem(cc, NC)) * n_tok, n_tok), n_tok)
 
-    def rec_part(j, carry):
+    block = 512
+
+    def out_part(j, carry):
         cols = pl.ds(pl.multiple_of(j * block, block), block)
-        pc[:, cols] += lax.dot_general(ro[...], orr[cols, :rw], NT_DIMS, preferred_element_type=f32)
+        pc[:, cols] = lax.dot_general(
+            co[...], oc[cols, :], NT_DIMS, preferred_element_type=f32
+        ) + lax.dot_general(ro[...], orr[cols, :rw], NT_DIMS, preferred_element_type=f32)
         for d in range(NX):
             ps[d, :, cols] = pc[chip_rows(x + d, c + 1), cols].astype(bf16)
         return carry
@@ -535,20 +528,20 @@
         lanes = lanes_of(q)
         return pltpu.make_async_remote_copy(
             src_ref=ps.at[d, :, lanes], dst_ref=pr.at[d, :, lanes],
-            send_sem=pr_s.at[4 * d + q], recv_sem=pr_r.at[4 * d + q],
+            send_sem=pr_s.at[0], recv_sem=pr_r.at[4 * d + q],
             device_id={"tp": x * NC + rem(c + 1, NC)}, device_id_type=MESH,
         )
 
     def project(q):
         n_blocks = quarter // block
-        lax.fori_loop(q * n_blocks, (q + 1) * n_blocks, rec_part, 0)
+        lax.fori_loop(q * n_blocks, (q + 1) * n_blocks, out_part, 0)
         for d in (2, 1, 3, 0):
             pair_copy(d, q).start()
 
     def x_copy(src, dst, index, q, xx):
         return pltpu.make_async_remote_copy(
             src_ref=src.at[:, lanes_of(q)], dst_ref=dst.at[:, lanes_of(q)],
-            send_sem=x_s.at[index], recv_sem=x_r.at[index],
+            send_sem=x_s.at[index // 4], recv_sem=x_r.at[index],
             device_id={"tp": rem(xx, NX) * NC + c}, device_id_type=MESH,
         )
 
@@ -600,21 +593,21 @@
 
     g_in.finish()
     g_out.finish()
-    for args in t_sent:
-        tok_copy(*args).wait_send()
+    tok_copy(nt.at[pl.ds(0, 7 * n_tok)], 0, x + 1, c).wait_send()
     for e in edges:
         e.wait_send()
-    for d in range(1, NX * NC):
-        stat_copy(d).wait_send()
-    for d in range(1, NY):
-        carry_copy(cy, y, cy_s, cy_r, d, (z, y + d)).wait_send()
-    for d in range(1, NZ):
-        carry_copy(cz, z, cz_s, cz_r, d, (z + d, y)).wait_send()
-    for q in range(4):
-        for d in range(NX):
-            pair_copy(d, q).wait_send()
-    for n in far + up + down:
-        n.wait_send()
+    stats_of_others.wait_send()
+    carry_copy(cy, pl.ds(0, NY - 1), cy_s, cy_r, (z, y + 1)).wait_send()
+    carry_copy(cz, pl.ds(0, NZ - 1), cz_s, cz_r, (z + 1, y)).wait_send()
+    pltpu.make_async_remote_copy(
+        src_ref=ps, dst_ref=pr, send_sem=pr_s.at[0], recv_sem=pr_r.at[0],
+        device_id={"tp": x * NC + rem(c + 1, NC)}, device_id_type=MESH,
+    ).wait_send()
+    for n, buf in enumerate((s2, sp_buf, sm_buf)):
+        pltpu.make_async_remote_copy(
+            src_ref=buf, dst_ref=two, send_sem=x_s.at[n], recv_sem=x_r.at[0],
+            device_id={"tp": rem(x + 1, NX) * NC + c}, device_id_type=MESH,
+        ).wait_send()
 
 
 def shards(
@@ -667,8 +660,8 @@
             V((n_tok, width), bf16),
             *Gather.semaphores(),
             *Gather.semaphores(),
-            S((9,)), S((9,)), S((2,)), S((2,)), S((7,)), S((7,)), S((3,)), S((3,)),
-            S((NZ - 1,)), S((NZ - 1,)), S((4 * NX,)), S((4 * NX,)), S((12,)), S((12,)),
+            S((1,)), S((9,)), S((2,)), S((2,)), S((1,)), S((1,)), S((1,)), S((1,)),
+            S((1,)), S((1,)), S((1,)), S((4 * NX,)), S((3,)), S((12,)),
         ],
         compiler_params=pltpu.CompilerParams(
             collective_id=0, has_side_effects=True, vmem_limit_bytes=60 * 1024 * 1024

time: 101 us -> 97.2 us (0.962)
  Pallas kernels: 99.4 us -> 95.2 us
    pallas_call x1, Pallas kernels: 99.4 us -> 95.2 us  [shards(): pl.pallas_call(whole_kernel, out_shape=jax.ShapeDtypeStruct((n_tok, width...]
where the time goes in v4:
time: 97.2 us; the launch traced here: 97 us
  Pallas kernels  95.2 us (98%)
  local copies, waits for them, and re-layouts  1.77 us (2%)
    pallas_call x1, Pallas kernels, shards(): pl.pallas_call(whole_kernel, out_shape=jax.ShapeDtypeStruct((n_tok, width...  95.2 us

profile of v4, /device:TPU:1, one launch (start us, length us, event | category | flops | bytes accessed | tf_op | source)
XLA Modules:
  0.0 97.0 jit_solution(13967526351733801762)
XLA Ops:
  0.0 95.2 %shard_map.154 = bf16[48,4096]{1,0:T(8,128)(2,1)} custom-call(bf16[48,4096]{1,0:T(8,128)(2,1)} %tokens.1, f32[1,4096]{1,0:T(1,128)} %bitcast.9, bf16[64,128]{1,0:T(8,128)(2,1)} %wv_own.1, bf16[64,128]{1,0:T(8,128)(2,1)} %wg_own.1, bf16[64,192]{1,0:T(8,128)(2,1)} %ri_own.1, bf16[64,192]{1,0:T(8,128)(2,1)} %rg_own.1, bf16[64,128]{1,0:T(8,128)(2,1)} %bitcast.10, ...), custom_call_target="tpu_custom_call" | custom-call | tf_op jit(solution)/shard_map/pallas_call | solution.py:624
  95.2 1.8 %copy.18 = bf16[48,4096]{1,0:T(8,128)(2,1)} copy(bf16[48,4096]{1,0:T(8,128)(2,1)} %shard_map.154) | data formatting | bytes 786432

commit v5 on v4

--- a/solution.py
+++ b/solution.py
@@ -66,10 +66,10 @@
 
     def spread(self, k):
         z, y = self.z, self.y
-        self.send(self.b, (z - k, y), 5, 3 * k, (z, y + 1))
-        self.send(self.b, (z - k, y), 5, 3 * k + 1, (z, y - 1))
+        self.send(self.b, (z - k, y), 5, 2 * k, (z, y + 1))
+        self.send(self.b, (z - k, y), 5, 2 * k, (z, y - 1))
         if k == HALF:
-            self.send(self.b, (z - k, y), 5, 3 * k + 2, (z, y + 2))
+            self.send(self.b, (z - k, y), 5, 2 * k + 1, (z, y + 2))
 
     def along_z(self, s, between=lambda: None):
         z, y, a, b = self.z, self.y, self.a, self.b
@@ -98,13 +98,16 @@
     def along_y(self, k):
         z, y = self.z, self.y
         turn = 1 - 2 * (k % 2)
-        self.arrived(self.b, (z - k, y - 1), 5, 3 * k)
-        self.arrived(self.b, (z - k, y + 1), 5, 3 * k + 1)
+        both = self.b.at[pl.ds(0, 2 * self.rows[id(self.b)])]
+        pltpu.make_async_remote_copy(
+            src_ref=both, dst_ref=both, send_sem=self.s[id(self.b)].at[0], recv_sem=self.r[5].at[2 * k],
+            device_id={"sp": rem(z + 1, NZ) * NY + y}, device_id_type=MESH,
+        ).wait_recv()
         if k != HALF:
-            self.send(self.b, (z - k, y - turn), 5, 3 * k + 2, (z, y + turn))
+            self.send(self.b, (z - k, y - turn), 5, 2 * k + 1, (z, y + turn))
 
     def along_y_last(self, k):
-        self.arrived(self.b, (self.z - k, self.y + 2), 5, 3 * k + 2)
+        self.arrived(self.b, (self.z - k, self.y + 2), 5, 2 * k + 1)
 
     def finish(self):
         for ref in (self.a, self.b):
@@ -116,7 +119,7 @@
 
     @staticmethod
     def semaphores():
-        counts = [1, 1, 3, 4 * HALF, 4 * HALF, HALF, HALF, 3 * NZ]
+        counts = [1, 1, 3, 4 * HALF, 4 * HALF, HALF, HALF, 2 * NZ]
         return [pltpu.SemaphoreType.DMA((n,)) for n in counts]
 
 
@@ -153,9 +156,15 @@
 SEGS = 8
 
 
-def whole_kernel(
-    tokens, gain, wv_own, wg_own, ri_own, rg_own, oc_own, or_own, taps, bias, cgain, staps, dmap, imap, base, jump_t, out, *scratch
-):
+def whole_kernel(*refs):
+    n_in = 16
+    given, out, scratch = refs[:n_in], refs[n_in], refs[n_in + 1 :]
+    held, in_sem, scratch = scratch[:n_in], scratch[n_in], scratch[n_in + 1 :]
+    loads = [pltpu.make_async_copy(g, h, in_sem.at[n]) for n, (g, h) in enumerate(zip(given, held))]
+    for load in loads:
+        load.start()
+    (tokens, gain, wv_own, wg_own, ri_own, rg_own, oc_own, or_own, taps, bias, cgain, staps, dmap, imap, base,
+     jump_t) = held
     (nt, wa, wb, acc_a, acc_b, oc, packed, orr, ext_c, ext_r, filt, md, mi, stats, dbuf, ibuf, gbuf, co, ro,
      jump, cy, cz, pc, ps, pr, s2, sp_buf, sm_buf, two, from_m, from_p) = scratch[:31]
     scratch = scratch[31:]
@@ -179,6 +188,8 @@
     for d in range(1, NX * NC):
         pl.semaphore_signal(barrier, inc=1, device_id={"tp": rem(tp + d, NX * NC)}, device_id_type=MESH)
 
+    for load in loads:
+        load.wait()
     own = pl.ds(pl.multiple_of(sp * rows, rows), rows)
     extra = wa.shape[1] - rw
     wa[own, :] = jnp.concatenate([ri_own[...], rg_own[:, :extra]], axis=1)
@@ -621,12 +632,32 @@
     f32, bf16 = jnp.float32, jnp.bfloat16
     vmem = pl.BlockSpec(memory_space=pltpu.VMEM)
     V, S = pltpu.VMEM, pltpu.SemaphoreType.DMA
+    given = (
+        tokens,
+        norm_gain[None, :],
+        conv_val_w,
+        conv_gate_w,
+        rec_in_w,
+        rec_gate_w,
+        out_conv_w.T,
+        out_rec_w.T,
+        conv_taps,
+        conv_bias[None, :],
+        conv_gain[None, :],
+        short_taps,
+        decay_map,
+        input_map,
+        decay_base[None, :],
+        decay_jump.T,
+    )
     return pl.pallas_call(
         whole_kernel,
-        out_shape=jax.ShapeDtypeStruct((n_tok, width), bf16),
-        in_specs=[vmem] * 16,
+        out_shape=pltpu.VMEM((n_tok, width), bf16),
+        in_specs=[pl.BlockSpec(memory_space=pltpu.HBM)] * 16,
         out_specs=vmem,
         scratch_shapes=[
+            *(V(g.shape, g.dtype) for g in given),
+            S((16,)),
             V((length, width), bf16),
             V((width, 2 * cw), bf16),
             V((width, 2 * rw), bf16),
@@ -664,26 +695,9 @@
             S((1,)), S((1,)), S((1,)), S((4 * NX,)), S((3,)), S((12,)),
         ],
         compiler_params=pltpu.CompilerParams(
-            collective_id=0, has_side_effects=True, vmem_limit_bytes=60 * 1024 * 1024
+            collective_id=0, has_side_effects=True, vmem_limit_bytes=66_640_000
         ),
-    )(
-        tokens,
-        norm_gain[None, :],
-        conv_val_w,
-        conv_gate_w,
-        rec_in_w,
-        rec_gate_w,
-        out_conv_w.T,
-        out_rec_w.T,
-        conv_taps,
-        conv_bias[None, :],
-        conv_gain[None, :],
-        short_taps,
-        decay_map,
-        input_map,
-        decay_base[None, :],
-        decay_jump.T,
-    )
+    )(*given)
 
 
 def solution(mesh):

time: 97.2 us -> 94.1 us (0.968)
  Pallas kernels: 95.2 us -> 93.2 us
  local copies, waits for them, and re-layouts: 1.77 us -> 0.75 us
    pallas_call x1, Pallas kernels: 95.2 us -> 93.2 us  [shards(): pl.pallas_call(whole_kernel, out_shape=pltpu.VMEM((n_tok, width), bf16),...]
    unnamed x1, local copies, waits for them, and re-layouts: 1.77 us -> 0.75 us
where the time goes in v5:
time: 94.1 us; the launch traced here: 93.9 us
  Pallas kernels  93.2 us (99%)
    pallas_call x1, Pallas kernels, shards(): pl.pallas_call(whole_kernel, out_shape=pltpu.VMEM((n_tok, width), bf16),...  93.2 us

profile of v5, /device:TPU:1, one launch (start us, length us, event | category | flops | bytes accessed | tf_op | source)
XLA Modules:
  0.0 93.9 jit_solution(8307769085238972972)
XLA Ops:
  0.0 93.2 %shard_map.154 = bf16[48,4096]{1,0:T(8,128)(2,1)S(1)} custom-call(bf16[48,4096]{1,0:T(8,128)(2,1)} %refs_0_.1, f32[1,4096]{1,0:T(1,128)} %bitcast.9, bf16[64,128]{1,0:T(8,128)(2,1)} %refs_2_.1, bf16[64,128]{1,0:T(8,128)(2,1)} %refs_3_.1, bf16[64,192]{1,0:T(8,128)(2,1)} %refs_4_.1, bf16[64,192]{1,0:T(8,128)(2,1)} %refs_5_.1, bf16[64,128]{1,0:T(8,128)(2,1)} %bitcast.10, ...), custom_call_target="tpu_custom_call" | custom-call | tf_op jit(solution)/shard_map/pallas_call | solution.py:653
  93.2 0.7 copy.18

commit v6 on v5

--- a/solution.py
+++ b/solution.py
@@ -417,7 +417,6 @@
     cy[y, :, half:] = s_run
     for d in range(1, NY):
         carry_copy(cy, pl.ds(y, 1), cy_s, cy_r, (z, y + d)).start()
-    out_step(HALF + 1 - lag)
     for k in groups_of(HALF):
         g_in.along_y(k)
     for k in groups_of(HALF - 1) + groups_of(HALF):
@@ -429,6 +428,7 @@
     edges[1].start()
     gate = jnp.concatenate([acc_a[:, rw:], acc_b[:, 2 * cw :]], axis=1).astype(bf16).astype(f32)
     gbuf[...] = 0.5 * gate * (1.0 + jnp.tanh(0.7978845608028654 * (gate + 0.044715 * gate * gate * gate)))
+    out_step(HALF + 1 - lag)
     carry_copy(cy, pl.ds(0, NY - 1), cy_s, cy_r, (z, y + 1)).wait_recv()
     p_run, s_run = jnp.ones((1, half), f32), jnp.zeros((1, half), f32)
     p_mine, s_mine = p_run, s_run

time: 94.1 us -> 93.6 us (level)
  no operation moved by 1% of the time
where the time goes in v6:
time: 93.6 us; the launch traced here: 93.5 us
  Pallas kernels  92.7 us (99%)
    pallas_call x1, Pallas kernels, shards(): pl.pallas_call(whole_kernel, out_shape=pltpu.VMEM((n_tok, width), bf16),...  92.7 us

profile of v6, /device:TPU:1, one launch (start us, length us, event | category | flops | bytes accessed | tf_op | source)
XLA Modules:
  0.0 93.5 jit_solution(2513214767550170412)
XLA Ops:
  0.0 92.7 %shard_map.154 = bf16[48,4096]{1,0:T(8,128)(2,1)S(1)} custom-call(bf16[48,4096]{1,0:T(8,128)(2,1)} %refs_0_.1, f32[1,4096]{1,0:T(1,128)} %bitcast.9, bf16[64,128]{1,0:T(8,128)(2,1)} %refs_2_.1, bf16[64,128]{1,0:T(8,128)(2,1)} %refs_3_.1, bf16[64,192]{1,0:T(8,128)(2,1)} %refs_4_.1, bf16[64,192]{1,0:T(8,128)(2,1)} %refs_5_.1, bf16[64,128]{1,0:T(8,128)(2,1)} %bitcast.10, ...), custom_call_target="tpu_custom_call" | custom-call | tf_op jit(solution)/shard_map/pallas_call | solution.py:653
  92.7 0.7 copy.18
